TPU v7x, 128 devices: a whole 4x4x4 slice. The times are simulated.
128 devices in a mesh: ep: 128 (over z, y, x, core).
Axes of the slice: x: 4, y: 4, z: 4, core: 2. Of those that a mesh axis runs over, the one named last changes fastest.
Arguments:
- hidden_in: bfloat16 [2048, 2048], P('ep'), may hold values from -6 to 6
- lengths: int32 [2048], P('ep'), may hold values from 1 to 1024
- attn_gain: float32 [2048], replicated, may hold values from 0.1 to 1.9
- query_weight: bfloat16 [2048, 512], replicated, may hold values from -0.125 to 0.125
- key_weight: bfloat16 [2048, 128], replicated, may hold values from -0.125 to 0.125
- value_weight: bfloat16 [2048, 128], replicated, may hold values from -0.125 to 0.125
- score_bias: float32 [8], replicated, may hold values from -7.5 to -3.5
- out_weight: bfloat16 [512, 2048], replicated, may hold values from -0.25 to 0.25
- key_cache: bfloat16 [2048, 1024, 128], P('ep'), may hold values from -6 to 6
- value_cache: bfloat16 [2048, 1024, 128], P('ep'), may hold values from -10 to 10
- ffn_gain: float32 [2048], replicated, may hold values from 0.1 to 1.9
- routes: int32 [2048, 4], P('ep'), may hold values from 0 to 127, all different within a row; in each aligned block of 16 rows (0 to 15, 16 to 31, ...) at most 1 rows name the same one
- route_weights: float32 [2048, 4], P('ep'), may hold values from 0.25 to 1
- expert_gate: bfloat16 [128, 2048, 512], P('ep'), may hold values from -0.125 to 0.125
- expert_up: bfloat16 [128, 2048, 512], P('ep'), may hold values from -0.125 to 0.125
- expert_down: bfloat16 [128, 512, 2048], P('ep'), may hold values from -0.25 to 0.25
- dense_gate: bfloat16 [2048, 2048], P(None, 'ep'), may hold values from -0.125 to 0.125
- dense_up: bfloat16 [2048, 2048], P(None, 'ep'), may hold values from -0.125 to 0.125
- dense_down: bfloat16 [2048, 2048], P(None, 'ep'), may hold values from -0.125 to 0.125
- branch_gate: float32 [2048], replicated, may hold values from -0.125 to 0.125
Outputs:
- hidden_out: bfloat16 [2048, 2048], P('ep')
- new_keys: bfloat16 [2048, 128], P('ep')
- new_values: bfloat16 [2048, 128], P('ep')
Inputs may be any that keep to these rules, and one draw needn't show every extreme that they name: `routes`: in each device's 16 rows no expert is named twice.
All inputs are finite; a program needn't handle non-finite values.
Results may differ from a plain program's by a relative error of at most 0.0061.
Values may be sent and summed in bfloat16 or wider, within the bound.
A program may use at most 128 MiB of HBM per device.

v0:
```python
import jax
import jax.numpy as jnp
from jax import lax
from jax.sharding import PartitionSpec as P

HEADS = 8
KV_HEADS = 2
HEAD = 64
TOP = 4


norm_eps = 1e-06


def turned_gather(arrays, axis, dims):
    turned = [jnp.moveaxis(a, dim, 0) for a, dim in zip(arrays, dims)]
    both = jnp.concatenate([t.reshape(len(t), -1) for t in turned], axis=1)
    result, at, done = (lax.all_gather(both, axis, axis=0, tiled=True), 0, [])
    for t, dim in zip(turned, dims):
        share = result[:, at : at + t[0].size].reshape(-1, *t.shape[1:])
        done.append(jnp.moveaxis(share, 0, dim))
        at += t[0].size
    return tuple(done)


def rms_norm(values_in, gain):
    as_float = values_in.astype(jnp.float32)
    scaled = as_float * lax.rsqrt(jnp.mean(as_float * as_float, axis=-1, keepdims=True) + norm_eps)
    return (scaled * gain).astype(jnp.bfloat16)


def later_sums(log_keep):
    cache_len = log_keep.shape[-1]
    span = 128
    block_count = cache_len // span
    lead_shape = log_keep.shape[:-1]
    blocked = log_keep.reshape(lead_shape + (block_count, span))
    span_pos = jnp.arange(span, dtype=jnp.int32)
    inner_tri = (span_pos[:, None] > span_pos[None, :]).astype(jnp.float32)
    inside = jnp.einsum("nkgbj,js->nkgbs", blocked, inner_tri, precision=lax.Precision.HIGHEST)
    totals = jnp.sum(blocked, axis=-1)
    block_pos = jnp.arange(block_count, dtype=jnp.int32)
    outer_tri = (block_pos[:, None] > block_pos[None, :]).astype(jnp.float32)
    beyond = jnp.einsum("nkgc,cb->nkgb", totals, outer_tri, precision=lax.Precision.HIGHEST)
    return (inside + beyond[..., None]).reshape(log_keep.shape)


def stick_attend(query_blk, key_blk, value_blk, seq_lens, score_bias):
    seq_count = query_blk.shape[0]
    cache_len = key_blk.shape[1]
    per_group = HEADS // KV_HEADS
    query_r = query_blk.reshape(seq_count, KV_HEADS, per_group, HEAD)
    key_r = key_blk.reshape(seq_count, cache_len, KV_HEADS, HEAD)
    value_r = value_blk.reshape(seq_count, cache_len, KV_HEADS, HEAD)
    head_bias = score_bias.reshape(KV_HEADS, per_group)[None, :, :, None]
    scores = jnp.einsum(
        "nkgd,nskd->nkgs", query_r, key_r, preferred_element_type=jnp.float32
    ) * HEAD ** (-0.5)
    scores = scores + head_bias
    live_mask = (jnp.arange(cache_len, dtype=jnp.int32)[None, :] < seq_lens[:, None])[
        :, None, None, :
    ]
    log_keep = jnp.where(live_mask, jax.nn.log_sigmoid(-scores), 0.0)
    after_sum = later_sums(log_keep)
    weights = jnp.where(live_mask, jnp.exp(jax.nn.log_sigmoid(scores) + after_sum), 0.0).astype(
        jnp.bfloat16
    )
    mixed = jnp.einsum("nkgs,nskd->nkgd", weights, value_r, preferred_element_type=jnp.float32)
    return mixed.astype(jnp.bfloat16).reshape(seq_count, HEADS * HEAD)


def dense_hidden_of(tok_rows, gate_w, up_w):
    gate_pre = jnp.dot(tok_rows, gate_w, preferred_element_type=jnp.float32)
    up_pre = jnp.dot(tok_rows, up_w, preferred_element_type=jnp.float32)
    return (jax.nn.silu(gate_pre) * up_pre).astype(jnp.bfloat16)


def down_product(hidden_rows, down_w):
    return lax.dot_general(
        hidden_rows, down_w, (((1,), (1,)), ((), ())), preferred_element_type=jnp.float32
    )


def per_device(
    hidden_in,
    lengths,
    attn_gain,
    query_weight,
    key_weight,
    value_weight,
    score_bias,
    out_weight,
    key_cache,
    value_cache,
    ffn_gain,
    routes,
    route_weights,
    expert_gate,
    expert_up,
    expert_down,
    dense_gate,
    dense_up,
    dense_down,
    branch_gate,
):
    seq_count = hidden_in.shape[0]
    row_width = hidden_in.shape[1]
    normed = rms_norm(hidden_in, attn_gain)
    queries = jnp.dot(normed, query_weight, preferred_element_type=jnp.float32).astype(jnp.bfloat16)
    new_keys = jnp.dot(normed, key_weight, preferred_element_type=jnp.float32).astype(jnp.bfloat16)
    new_values = jnp.dot(normed, value_weight, preferred_element_type=jnp.float32).astype(
        jnp.bfloat16
    )
    attended = stick_attend(queries, key_cache, value_cache, lengths, score_bias)
    middle = hidden_in.astype(jnp.float32) + jnp.dot(
        attended, out_weight, preferred_element_type=jnp.float32
    )
    ffn_in = rms_norm(middle, ffn_gain)
    devices = lax.axis_size("ep")
    local_experts = expert_gate.shape[0]
    experts_all = local_experts * devices
    capacity = max(1, seq_count * TOP // experts_all)
    flat_ids = routes.reshape(-1)
    pick_count = flat_ids.shape[0]
    pick_pos = jnp.arange(pick_count, dtype=jnp.int32)
    same_expert = (flat_ids[:, None] == flat_ids[None, :]) & (pick_pos[None, :] < pick_pos[:, None])
    slot_rank = jnp.sum(same_expert.astype(jnp.int32), axis=1)
    slot_index = flat_ids * capacity + slot_rank
    pick_rows = jnp.repeat(ffn_in, TOP, axis=0)
    outgoing = (
        jnp.zeros((experts_all * capacity, row_width), jnp.bfloat16).at[slot_index].set(pick_rows)
    )
    outgoing = outgoing.reshape(devices, local_experts * capacity, row_width)
    arrived = lax.all_to_all(outgoing, "ep", split_axis=0, concat_axis=0, tiled=True)
    flat_in = arrived.reshape(-1, row_width)
    gate_pre = jnp.dot(flat_in, expert_gate[0], preferred_element_type=jnp.float32)
    up_pre = jnp.dot(flat_in, expert_up[0], preferred_element_type=jnp.float32)
    hidden_act = (jax.nn.silu(gate_pre) * up_pre).astype(jnp.bfloat16)
    expert_rows = jnp.dot(hidden_act, expert_down[0], preferred_element_type=jnp.float32).astype(
        jnp.bfloat16
    )
    returned = lax.all_to_all(
        expert_rows.reshape(arrived.shape), "ep", split_axis=0, concat_axis=0, tiled=True
    )
    returned = returned.reshape(experts_all * capacity, row_width)
    picked = returned[slot_index].reshape(seq_count, TOP, row_width).astype(jnp.float32)
    expert_sum = jnp.sum(picked * route_weights[:, :, None], axis=1)
    full_gate, full_up, full_down = turned_gather(
        (dense_gate, dense_up, dense_down), "ep", (1, 1, 1)
    )
    dense_out = down_product(dense_hidden_of(ffn_in, full_gate, full_up), full_down)
    gate_value = jax.nn.sigmoid(
        jnp.dot(ffn_in.astype(jnp.float32), branch_gate, precision=lax.Precision.HIGHEST)
    )
    hidden_out = (middle + expert_sum + gate_value[:, None] * dense_out).astype(jnp.bfloat16)
    return (hidden_out, new_keys, new_values)


def solution(mesh):
    return jax.shard_map(
        per_device,
        mesh=mesh,
        in_specs=(
            P("ep", None),
            P("ep"),
            P(),
            P(),
            P(),
            P(),
            P(),
            P(),
            P("ep", None, None),
            P("ep", None, None),
            P(),
            P("ep", None),
            P("ep", None),
            P("ep", None, None),
            P("ep", None, None),
            P("ep", None, None),
            P(None, "ep"),
            P(None, "ep"),
            P(None, "ep"),
            P(),
        ),
        out_specs=(P("ep", None), P("ep", None), P("ep", None)),
        check_vma=False,
    )
```

profile of v0, /device:TPU:1, one launch (start us, length us, event | category | flops | bytes accessed | tf_op | source)
XLA Modules:
  0.0 139.7 jit_solution(4658724207603570071)
XLA Ops:
  7.2 1.7 %pad_maximum_fusion = bf16[16,6144]{1,0:T(8,128)(2,1)} fusion(bf16[16,2048]{1,0:T(8,128)(2,1)} %bitcast.78, bf16[16,2048]{1,0:T(8,128)(2,1)} %bitcast.79, bf16[16,2048]{1,0:T(8,128)(2,1)} %bitcast.80), kind=kLoop, calls=%fused_computation.59 | loop fusion | flops 589824 | bytes 393216 | tf_op jit(solution)/shard_map/concatenate | solution.py:17
  10.9 2.1 %convolution_convert_fusion.2 = bf16[16,512]{1,0:T(8,128)(2,1)S(1)} fusion(bf16[2048,512]{1,0:T(8,128)(2,1)} %param.23, bf16[16,2048]{1,0:T(8,128)(2,1)} %param.20, f32[2048]{0:T(1024)} %param.22, f32[16]{0:T(128)S(1)} %add_rsqrt_fusion.1), kind=kOutput, calls=%fused_computation.29 | convolution fusion | flops 33693696 | bytes 2187328 | tf_op jit(solution)/shard_map/dot_general | solution.py:109
  13.1 6.4 %copy.52 = bf16[16,1024,128]{1,2,0:T(8,128)(2,1)} copy(bf16[16,1024,128]{2,1,0:T(8,128)(2,1)} %param.28) | data formatting | bytes 8388608 | tf_op args[8]
  19.7 4.0 %fusion.48 = (f32[16,2,4,1024]{3,2,1,0:T(4,128)S(1)}, f32[16,2,4,1024]{3,2,1,0:T(4,128)}) fusion(pred[16,1024]{1,0:T(8,128)(4,1)S(1)} %iota_compare_fusion.1, f32[2,4]{1,0:T(2,128)S(1)} %add.87, bf16[16,2,4,64]{3,2,1,0:T(4,128)(2,1)S(1)} %reshape.109, bf16[16,1024,2,64]{1,3,2,0:T(8,128)(2,1)} %bitcast.75), kind=kOutput, calls=%fused_computation.43 | convolution fusion | flops 18087936 | bytes 5275680 | tf_op jit(solution)/shard_map/nkgd,nskd->nkgs/dot_general | solution.py:56
  25.2 6.4 %copy.55 = bf16[16,1024,128]{1,2,0:T(8,128)(2,1)} copy(bf16[16,1024,128]{2,1,0:T(8,128)(2,1)} %param.29) | data formatting | bytes 8388608 | tf_op args[9]
  31.7 3.6 %convolution_convert_fusion.1 = bf16[16,2,4,64]{3,2,1,0:T(4,128)(2,1)S(1)} fusion(bf16[16,1024,2,64]{1,3,2,0:T(8,128)(2,1)} %bitcast.76, f32[16,2,4,1024]{3,2,1,0:T(4,128)S(1)} %reshape.112, f32[16,2,4,1024]{3,2,1,0:T(4,128)} %get-tuple-element.4, pred[16,1024]{1,0:T(8,128)(4,1)S(1)} %iota_compare_fusion.1), kind=kOutput, calls=%fused_computation.28 | convolution fusion | flops 18227200 | bytes 5275648 | tf_op jit(solution)/shard_map/nkgs,nskd->nkgd/dot_general | solution.py:68
  35.4 2.1 %multiply_reduce_fusion.1 = (f32[16]{0:T(128)S(1)}, f32[16,2048]{1,0:T(8,128)S(1)}) fusion(bf16[16,512]{1,0:T(8,128)(2,1)S(1)} %reshape.114, bf16[512,2048]{1,0:T(8,128)(2,1)} %param.27, bf16[16,2048]{1,0:T(8,128)(2,1)S(1)} %copy-done.1), kind=kOutput, calls=%fused_computation.72 | convolution fusion | flops 33685488 | bytes 2310208 | tf_op jit(solution)/shard_map/dot_general | solution.py:115
  40.6 1.2 reshape.144
  41.9 11.9 %all-to-all-start = ((bf16[128,2,1024]{2,1,0:T(2,128)(2,1)}), bf16[128,2,1024]{2,1,0:T(2,128)(2,1)}, u32[]{:S(2)}, u32[]{:S(2)}) async-start(bf16[128,2,1024]{2,1,0:T(2,128)(2,1)} %reshape.144), calls=%async_computation | async-start | bytes 1048576 | tf_op jit(solution)/shard_map/all_to_all | solution.py:134
  54.5 14.4 %all-to-all-done = bf16[128,2,1024]{2,1,0:T(2,128)(2,1)} async-done(((bf16[128,2,1024]{2,1,0:T(2,128)(2,1)}), bf16[128,2,1024]{2,1,0:T(2,128)(2,1)}, u32[]{:S(2)}, u32[]{:S(2)}) %all-to-all-start) | async-done | bytes 524320 | tf_op jit(solution)/shard_map/all_to_all | solution.py:134
  68.9 3.6 %reshape.145 = bf16[128,1,2048]{2,1,0:T(2,128)(2,1)S(1)} reshape(bf16[128,2,1024]{2,1,0:T(2,128)(2,1)} %all-to-all-done) | data formatting | bytes 1048576
  72.5 2.7 %fusion.27 = f32[128,512]{1,0:T(8,128)S(1)} fusion(bf16[1,2048,512]{2,1,0:T(8,128)(2,1)} %param.33, bf16[128,1,2048]{2,1,0:T(2,128)(2,1)S(1)} %reshape.145), kind=kOutput, calls=%fused_computation.19 | convolution fusion | flops 268435456 | bytes 2883584 | tf_op jit(solution)/shard_map/dot_general | solution.py:136
  75.3 3.4 %fusion.6 = bf16[128,1,2048]{2,0,1:T(8,128)(2,1)} fusion(bf16[1,512,2048]{2,1,0:T(8,128)(2,1)S(1)} %copy-done, bf16[1,2048,512]{2,1,0:T(8,128)(2,1)} %param.34, f32[128,512]{1,0:T(8,128)S(1)} %fusion.27, bf16[128,1,2048]{2,1,0:T(2,128)(2,1)S(1)} %reshape.145), kind=kOutput, calls=%fused_computation.9 | convolution fusion | flops 537526272 | bytes 5505024 | tf_op jit(solution)/shard_map/dot_general | solution.py:139
  78.6 2.0 %reduce.1 = bf16[128,2048]{1,0:T(8,128)(2,1)S(1)} reduce(bf16[128,1,2048]{2,0,1:T(8,128)(2,1)} %fusion.6, bf16[]{:T(256)} %broadcast.85), dimensions={1}, to_apply=%copy.59.reduce_sub_computation | reduce | bytes 1048578 | tf_op jit(solution)/shard_map/reshape | solution.py:143
  80.7 1.2 reshape.146
  81.9 4.0 %all-to-all-start.1 = ((bf16[128,2,1024]{2,1,0:T(2,128)(2,1)}), bf16[128,2,1024]{2,1,0:T(2,128)(2,1)S(1)}, u32[]{:S(2)}, u32[]{:S(2)}) async-start(bf16[128,2,1024]{2,1,0:T(2,128)(2,1)} %reshape.146), calls=%async_computation.1 | async-start | bytes 1048576 | tf_op jit(solution)/shard_map/all_to_all | solution.py:142
  86.7 2.0 %convolution_convert_fusion.3 = bf16[16,128]{1,0:T(8,128)(2,1)} fusion(bf16[2048,128]{1,0:T(8,128)(2,1)} %param.25, bf16[16,2048]{1,0:T(8,128)(2,1)S(1)} %copy-done.1, f32[2048]{0:T(1024)S(1)} %copy-done.4, f32[16]{0:T(128)S(1)} %add_rsqrt_fusion.1), kind=kOutput, calls=%fused_computation.30 | convolution fusion | flops 8521728 | bytes 602176 | tf_op jit(solution)/shard_map/dot_general | solution.py:111
  88.7 1.9 %convolution_convert_fusion.4 = bf16[16,128]{1,0:T(8,128)(2,1)} fusion(bf16[2048,128]{1,0:T(8,128)(2,1)} %param.24, bf16[16,2048]{1,0:T(8,128)(2,1)S(1)} %copy-done.1, f32[2048]{0:T(1024)S(1)} %copy-done.4, f32[16]{0:T(128)S(1)} %add_rsqrt_fusion.1), kind=kOutput, calls=%fused_computation.31 | convolution fusion | flops 8521728 | bytes 602176 | tf_op jit(solution)/shard_map/dot_general | solution.py:110
  90.6 15.0 %all-to-all-done.1 = bf16[128,2,1024]{2,1,0:T(2,128)(2,1)S(1)} async-done(((bf16[128,2,1024]{2,1,0:T(2,128)(2,1)}), bf16[128,2,1024]{2,1,0:T(2,128)(2,1)S(1)}, u32[]{:S(2)}, u32[]{:S(2)}) %all-to-all-start.1) | async-done | bytes 524320 | tf_op jit(solution)/shard_map/all_to_all | solution.py:142
  105.6 1.8 %reshape.147 = bf16[128,1,2048]{2,1,0:T(2,128)(2,1)} reshape(bf16[128,2,1024]{2,1,0:T(2,128)(2,1)S(1)} %all-to-all-done.1) | data formatting | bytes 1048576
  107.3 1.5 %copy.77 = bf16[128,1,2048]{2,0,1:T(8,128)(2,1)S(1)} copy(bf16[128,1,2048]{2,1,0:T(2,128)(2,1)} %reshape.147) | data formatting | bytes 1048576
  110.2 7.2 %all-gather.2.cloned.1.call-done = bf16[2048,6144]{1,0:T(8,128)(2,1)} async-done(((bf16[16,6144]{1,0:T(8,128)(2,1)}), bf16[2048,6144]{1,0:T(8,128)(2,1)}) %all-gather.2.cloned.1.call-update) | async-done | bytes 25165840 | tf_op jit(solution)/shard_map/all_gather | solution.py:18
  117.4 5.6 %fusion.4 = f32[16,2048]{1,0:T(8,128)S(1)} fusion(bf16[16,2048]{1,0:T(8,128)(2,1)S(1)} %multiply_convert_fusion, bf16[2048,6144]{1,0:T(8,128)(2,1)} %all-gather.2.cloned.1.call-done), kind=kOutput, calls=%fused_computation.6 | convolution fusion | flops 134217728 | bytes 8585216 | tf_op jit(solution)/shard_map/dot_general | solution.py:73
  123.0 9.8 %fusion.19 = bf16[16,2048]{1,0:T(8,128)(2,1)} fusion(bf16[2048,6144]{1,0:T(8,128)(2,1)} %all-gather.2.cloned.1.call-done, bf16[16,2048]{1,0:T(8,128)(2,1)S(1)} %multiply_convert_fusion, f32[16,2048]{1,0:T(8,128)S(1)} %fusion.4, f32[16,2048]{1,0:T(8,128)S(1)} %copy-done.3, f32[16,2048]{1,0:T(8,128)S(1)} %multiply_reduce_fusion, f32[16]{0:T(128)S(1)} %copy-done.11), kind=kOutput, calls=%fused_computation.15 | convolution fusion | flops 268763136 | bytes 17301568 | tf_op jit(solution)/shard_map/dot_general | solution.py:79
  (56 shorter events, 9.7 us)
Async XLA Ops:
  7.2 68.1 %copy-start = (bf16[1,512,2048]{2,1,0:T(8,128)(2,1)S(1)}, bf16[1,512,2048]{2,1,0:T(8,128)(2,1)}, u32[]{:S(2)}) copy-start(bf16[1,512,2048]{2,1,0:T(8,128)(2,1)} %param.35) | copy-start | bytes 6291460
  7.2 110.2 %all-gather.2.cloned.1.call-start = ((), (), s32[]{:S(2)}) async-start(), calls=%async_computation.2 | async-start | bytes 25362432 | tf_op jit(solution)/shard_map/all_gather | solution.py:18
  13.1 6.4 %copy-start.10 = (f32[8]{0:T(128)S(1)}, f32[8]{0:T(128)}, u32[]{:S(2)}) copy-start(f32[8]{0:T(128)} %param.26) | copy-start | bytes 100
  13.1 6.5 %copy-start.7 = (s32[16]{0:T(128)S(1)}, s32[16]{0:T(128)}, u32[]{:S(2)}) copy-start(s32[16]{0:T(128)} %param.21) | copy-start | bytes 196
  31.7 3.7 %copy-start.1 = (bf16[16,2048]{1,0:T(8,128)(2,1)S(1)}, bf16[16,2048]{1,0:T(8,128)(2,1)}, u32[]{:S(2)}) copy-start(bf16[16,2048]{1,0:T(8,128)(2,1)} %param.20) | copy-start | bytes 196612
  31.7 5.8 %copy-start.5 = (f32[2048]{0:T(1024)S(1)}, f32[2048]{0:T(1024)}, u32[]{:S(2)}) copy-start(f32[2048]{0:T(1024)} %param.30) | copy-start | bytes 24580
  35.3 18.5 %copy-start.9 = (f32[2048]{0:T(1024)S(1)}, f32[2048]{0:T(1024)}, u32[]{:S(2)}) copy-start(f32[2048]{0:T(1024)} %param.39) | copy-start | bytes 24580
  37.5 31.4 %copy-start.2 = (f32[16,2048]{1,0:T(8,128)}, f32[16,2048]{1,0:T(8,128)S(1)}, u32[]{:S(2)}) copy-start(f32[16,2048]{1,0:T(8,128)S(1)} %get-tuple-element.6) | copy-start | bytes 393220
  38.0 34.5 %copy-start.8 = (s32[64]{0:T(128)}, s32[64]{0:T(128)S(1)}, u32[]{:S(2)}) copy-start(s32[64]{0:T(128)S(1)} %fusion.82) | copy-start | bytes 772
  41.9 27.0 %all-to-all-start = ((bf16[128,2,1024]{2,1,0:T(2,128)(2,1)}), bf16[128,2,1024]{2,1,0:T(2,128)(2,1)}, u32[]{:S(2)}, u32[]{:S(2)}) async-start(bf16[128,2,1024]{2,1,0:T(2,128)(2,1)} %reshape.144), calls=%async_computation | async-start | bytes 1048576 | tf_op jit(solution)/shard_map/all_to_all | solution.py:134
  75.2 11.4 %copy-start.6 = (f32[16,4]{0,1:T(4,128)S(1)}, f32[16,4]{0,1:T(4,128)}, u32[]{:S(2)}) copy-start(f32[16,4]{0,1:T(4,128)} %param.32) | copy-start | bytes 772
  75.3 11.4 %copy-start.4 = (f32[2048]{0:T(1024)S(1)}, f32[2048]{0:T(1024)}, u32[]{:S(2)}) copy-start(f32[2048]{0:T(1024)} %param.22) | copy-start | bytes 24580
  81.9 23.7 %all-to-all-start.1 = ((bf16[128,2,1024]{2,1,0:T(2,128)(2,1)}), bf16[128,2,1024]{2,1,0:T(2,128)(2,1)S(1)}, u32[]{:S(2)}, u32[]{:S(2)}) async-start(bf16[128,2,1024]{2,1,0:T(2,128)(2,1)} %reshape.146), calls=%async_computation.1 | async-start | bytes 1048576 | tf_op jit(solution)/shard_map/all_to_all | solution.py:142
  110.2 12.8 %copy-start.3 = (f32[16,2048]{1,0:T(8,128)S(1)}, f32[16,2048]{1,0:T(8,128)}, u32[]{:S(2)}) copy-start(f32[16,2048]{1,0:T(8,128)} %copy-done.2) | copy-start | bytes 393220
  110.2 12.8 %copy-start.11 = (f32[16]{0:T(128)S(1)}, f32[16]{0:T(128)}, u32[]{:S(2)}) copy-start(f32[16]{0:T(128)} %fusion.39) | copy-start | bytes 196
Sparse Core Ops, SparseCore 0:
  11.1 106.2 all-gather.1
where the time goes:
time: 141 us; the launch traced here: 140 us
  matrix products  38.7 us (27%)
  waiting for transfers between devices  36.5 us (26%)
  local copies, waits for them, and re-layouts  26.8 us (19%)
  starting transfers between devices  16 us (11%)
  between operations  14.3 us (10%)
  other arithmetic  7.42 us (5%)
    unnamed x33, local copies, waits for them, and re-layouts  23.1 us
    all_to_all x1, waiting for transfers between devices, per_device(): lax.all_to_all(expert_rows.reshape(arrived.shape), 'ep', split_axis=0, co...  15 us
    all_to_all x1, waiting for transfers between devices, per_device(): lax.all_to_all(outgoing, 'ep', split_axis=0, concat_axis=0, tiled=True)  14.4 us
    all_to_all x1, starting transfers between devices, per_device(): lax.all_to_all(outgoing, 'ep', split_axis=0, concat_axis=0, tiled=True)  11.9 us
    dot_general x1, matrix products, down_product(): lax.dot_general(hidden_rows, down_w, (((1,), (1,)), ((), ())), preferred_...  9.79 us
    all_gather x1, waiting for transfers between devices, turned_gather(): result, at, done = (lax.all_gather(both, axis, axis=0, tiled=True), 0, [])  7.15 us
    dot_general x1, matrix products, dense_hidden_of(): gate_pre = jnp.dot(tok_rows, gate_w, preferred_element_type=jnp.float32)  5.64 us
    dot_general x1, matrix products, stick_attend(): jnp.einsum('nkgd,nskd->nkgs', query_r, key_r, preferred_element_type=jnp....  4.05 us
  transfers between devices with their start and end apart: 3, of which 3 were waited for; matrix products, arithmetic and copies ran while one was open for 40% of the time, Pallas kernels for 0%

commit v1 on v0

v1 whole, which is shorter than its diff:
```python
import jax
import jax.numpy as jnp
from jax import lax
from jax.experimental import pallas as pl
from jax.experimental.pallas import tpu as pltpu
from jax.sharding import PartitionSpec as P

AXIS = "ep"
DEV = 128
GROUP = 8
RING = 4
SEQ = 16
D = 2048
LEN = 1024
HEAD = 64
HEADS = 8
TOP = 4
EFF = 512
UNITS = 16
CHUNK = 4
EPS = 1e-06
MESH = pl.DeviceIdType.MESH
BF16 = jnp.bfloat16
F32 = jnp.float32


def rms_norm(values, gain):
    scale = lax.rsqrt(jnp.mean(values * values, axis=-1, keepdims=True) + EPS)
    return (values * scale * gain).astype(BF16)


def silu(v):
    return v / (1.0 + jnp.exp(-v))


def nt_dot(a, b):
    return lax.dot_general(a, b, (((1,), (1,)), ((), ())), preferred_element_type=F32)


def dot(a, b):
    return jnp.dot(a, b, preferred_element_type=F32)


def kernel(
    lens,
    bias,
    routes,
    route_weights,
    hid,
    attn_gain,
    ffn_gain,
    branch_gate,
    routes_v,
    qw_h,
    kw_h,
    vw_h,
    ow_h,
    kc_h,
    vc_h,
    eg_h,
    eu_h,
    ed_h,
    dg_h,
    du_h,
    dd_h,
    out,
    new_keys,
    new_values,
    qw,
    kw,
    vw,
    ow,
    kc,
    vc,
    eg,
    eu,
    ed,
    wbuf,
    xg,
    part,
    parts_in,
    tile32,
    send1,
    arr1,
    send2,
    arr2,
    qs,
    os_,
    tri,
    mid_s,
    w_sem,
    k_sem,
    v_sem,
    e_sem,
    d_sem,
    snd,
    rcv,
):
    me = lax.axis_index(AXIS)
    grp = me // GROUP
    mem = lax.rem(me, GROUP)
    zz = grp // RING
    yy = lax.rem(grp, RING)

    def copy(src, dst, sem):
        return pltpu.make_async_copy(src, dst, sem)

    own = [
        copy(dg_h, wbuf.at[zz, yy, pl.ds(0, UNITS)], d_sem.at[0]),
        copy(du_h, wbuf.at[zz, yy, pl.ds(UNITS, UNITS)], d_sem.at[1]),
        copy(dd_h, wbuf.at[zz, yy, pl.ds(2 * UNITS, UNITS)], d_sem.at[2]),
    ]
    proj = [copy(qw_h, qw, w_sem.at[0]), copy(kw_h, kw, w_sem.at[1]), copy(vw_h, vw, w_sem.at[2])]
    outw = [
        copy(
            ow_h.at[pl.ds(h * HEAD, HEAD)],
            ow.at[pl.ds((h % 4) * 2 * HEAD + (h // 4) * HEAD, HEAD)],
            w_sem.at[3 + h],
        )
        for h in range(HEADS)
    ]
    experts = [copy(eg_h.at[0], eg, e_sem.at[0]), copy(eu_h.at[0], eu, e_sem.at[1]), copy(ed_h.at[0], ed, e_sem.at[2])]
    for c in proj + own:
        c.start()

    barrier = pltpu.get_barrier_semaphore()

    @pl.loop(1, DEV)
    def _(d):
        pl.semaphore_signal(barrier, inc=1, device_id=(lax.rem(me + d, DEV),), device_id_type=MESH)

    @pl.loop(0, SEQ)
    def _(b):
        copy(kc_h.at[b], kc.at[b], k_sem.at[b]).start()
        copy(vc_h.at[b], vc.at[b], v_sem.at[b]).start()

    for c in outw + experts:
        c.start()

    row = lax.broadcasted_iota(jnp.int32, (128, 256), 0)
    col = lax.broadcasted_iota(jnp.int32, (128, 256), 1)
    tri[...] = jnp.where((row > col) | (col >= 128), 1.0, 0.0).astype(BF16)

    normed = rms_norm(hid[...].astype(F32), attn_gain[...])
    for c in proj:
        c.wait()
    new_keys[...] = dot(normed, kw[...]).astype(BF16)
    new_values[...] = dot(normed, vw[...]).astype(BF16)
    queries = dot(normed, qw[...]).astype(BF16).astype(F32)
    low = lax.broadcasted_iota(jnp.int32, (SEQ, 128), 1) < HEAD
    for h in range(HEADS):
        piece = queries[:, (h // 2) * 128 : (h // 2 + 1) * 128]
        if (h % 2) != (h // 4):
            piece = pltpu.roll(piece, HEAD, axis=1)
        piece = jnp.where(low, piece, 0.0) if h < 4 else jnp.where(low, 0.0, piece)
        qs[pl.ds(h, SEQ, stride=HEADS), :] = piece

    pl.semaphore_wait(barrier, DEV - 1)
    for c in own:
        c.wait()
    half = D // 2
    left, right = pl.ds(0, half), pl.ds(half, half)

    def device(z, y, member):
        return ((z * RING + y) * GROUP + member,)

    def remote(src, dst, s, to):
        return pltpu.make_async_remote_copy(
            src_ref=src, dst_ref=dst, send_sem=snd.at[s], recv_sem=rcv.at[s], device_id=to, device_id_type=MESH
        )

    for d in (1, 3, 2):
        a = wbuf.at[zz, yy, :, left]
        remote(a, a, 0, device(zz, lax.rem(yy + d, RING), mem)).start()
        b = wbuf.at[zz, yy, :, right]
        remote(b, b, 1, device(lax.rem(zz + d, RING), yy, mem)).start()

    heads = lax.broadcasted_iota(jnp.int32, (HEADS, LEN), 0)
    bias_v = jnp.zeros((HEADS, LEN), F32)
    for h in range(HEADS):
        bias_v = jnp.where(heads == h, bias[h], bias_v)
    pos = lax.broadcasted_iota(jnp.int32, (HEADS, LEN), 1)
    blocks = LEN // 128

    @pl.loop(0, SEQ // CHUNK)
    def _(i):
        logs, keeps, lives = [], [], []
        for j in range(CHUNK):
            b = i * CHUNK + j
            copy(kc_h.at[b], kc.at[b], k_sem.at[b]).wait()
            q = qs[pl.ds(pl.multiple_of(b * HEADS, HEADS), HEADS), :].astype(BF16)
            z = nt_dot(q, kc[b]) * (HEAD**-0.5) + bias_v
            live = pos < lens[b]
            t = jnp.log(1.0 + jnp.exp(-jnp.abs(z)))
            logs.append(jnp.minimum(z, 0.0) - t)
            keeps.append(jnp.where(live, jnp.minimum(-z, 0.0) - t, 0.0))
            lives.append(live)
        keep = jnp.concatenate(
            [keeps[j][:, c * 128 : (c + 1) * 128] for j in range(CHUNK) for c in range(blocks)], axis=0
        )
        hi = keep.astype(BF16)
        rest = keep - hi.astype(F32)
        mid = rest.astype(BF16)
        lo = (rest - mid.astype(F32)).astype(BF16)
        sums = dot(hi, tri[...]) + dot(mid, tri[...]) + dot(lo, tri[...])
        for j in range(CHUNK):
            b = i * CHUNK + j
            beyond = jnp.zeros((HEADS, 128), F32)
            pieces = [None] * blocks
            for c in reversed(range(blocks)):
                at = (j * blocks + c) * HEADS
                after = sums[at : at + HEADS, :128] + beyond
                beyond = beyond + sums[at : at + HEADS, 128:]
                cut = slice(c * 128, (c + 1) * 128)
                pieces[c] = jnp.where(lives[j][:, cut], jnp.exp(logs[j][:, cut] + after), 0.0)
            weights = jnp.concatenate(pieces, axis=1).astype(BF16)
            copy(vc_h.at[b], vc.at[b], v_sem.at[b]).wait()
            os_[pl.ds(pl.multiple_of(b * HEADS, HEADS), HEADS), :] = dot(weights, vc[b])

    for c in outw:
        c.wait()
    attended = []
    for h in range(4):
        first = os_[pl.ds(h, SEQ, stride=HEADS), :]
        second = os_[pl.ds(h + 4, SEQ, stride=HEADS), :]
        attended.append(jnp.where(low, first, second).astype(BF16))
    middle = hid[...].astype(F32) + dot(jnp.concatenate(attended, axis=1), ow[...])
    mid_s[...] = middle
    ffn_in = rms_norm(middle, ffn_gain[...])
    mine = pl.ds(pl.multiple_of(mem * SEQ, SEQ), SEQ)
    xg[mine, :] = ffn_in

    experts_i = lax.broadcasted_iota(jnp.int32, (DEV, SEQ), 0)
    hit = routes_v[0:1, :] == experts_i
    for k in range(1, TOP):
        hit = hit | (routes_v[k : k + 1, :] == experts_i)
    pick = jnp.where(hit, 1.0, 0.0).astype(BF16)

    def to_rows(values, c):
        for j in range(values.shape[1] // 128):
            tile32[pl.ds(c + j, DEV, stride=16), :] = values[:, j * 128 : (j + 1) * 128]

    def pack(dst):
        @pl.loop(0, DEV // 8)
        def _(i):
            for j in range(8):
                r = i * 8 + j
                dst[r] = tile32[pl.ds(pl.multiple_of(r * 16, 16), 16), :].astype(BF16)

    def exchange(src, dst, s):
        @pl.loop(1, DEV)
        def _(d):
            t = lax.rem(me + d, DEV)
            remote(src.at[t], dst.at[me], s, (t,)).start()

    def waited(ref, s):
        copy(ref, ref, snd.at[s]).wait()

    def arrived(ref, s):
        copy(ref, ref, rcv.at[s]).wait()

    for c in range(0, 16, 4):
        to_rows(dot(pick, ffn_in[:, c * 128 : (c + 4) * 128]), c)
    pack(send1)
    exchange(send1, arr1, 2)
    arr1[me] = send1[me]
    for d in (1, 2, 3, 4, 5, 6, 7):
        to = lax.rem(mem + d, GROUP)
        remote(xg.at[mine], xg.at[mine], 3, device(zz, yy, to)).start()

    a_in = wbuf.at[zz, pl.ds(0, RING - 1), :, left]
    b_in = wbuf.at[pl.ds(0, RING - 1), yy, :, right]
    arrived(a_in, 0)
    arrived(b_in, 1)
    for d in (1, 3, 2):
        a = wbuf.at[zz, :, :, left]
        remote(a, a, 4, device(lax.rem(zz + d, RING), yy, mem)).start()
        b = wbuf.at[:, yy, :, right]
        remote(b, b, 5, device(zz, lax.rem(yy + d, RING), mem)).start()

    for c in experts:
        c.wait()
    most = pl.ds(0, DEV - 1)
    arrived(arr1.at[most], 2)

    @pl.loop(0, DEV // 8)
    def _(i):
        for j in range(8):
            r = i * 8 + j
            tile32[pl.ds(pl.multiple_of(r * 16, 16), 16), :] = arr1[r].astype(F32)

    rows = jnp.concatenate([tile32[pl.ds(c, DEV, stride=16), :].astype(BF16) for c in range(16)], axis=1)
    hidden = (silu(dot(rows, eg[...])) * dot(rows, eu[...])).astype(BF16)
    for c in range(0, 16, 4):
        to_rows(dot(hidden, ed[:, c * 128 : (c + 4) * 128]), c)
    pack(send2)
    exchange(send2, arr2, 6)
    arr2[me] = send2[me]

    arrived(xg.at[pl.ds(0, SEQ * (GROUP - 1))], 3)
    arrived(wbuf.at[pl.ds(0, RING - 1), :, :, left], 4)
    arrived(wbuf.at[:, pl.ds(0, RING - 1), :, right], 5)
    tokens = xg[...]

    def share(n):
        return wbuf[:, :, n * UNITS : (n + 1) * UNITS, :].reshape(RING * RING * UNITS, D)

    dense_hidden = (silu(nt_dot(tokens, share(0))) * nt_dot(tokens, share(1))).astype(BF16)
    part[...] = dot(dense_hidden, share(2)).astype(BF16)
    for d in range(1, GROUP):
        to = lax.rem(mem + d, GROUP)
        theirs = pl.ds(pl.multiple_of(to * SEQ, SEQ), SEQ)
        remote(part.at[theirs], parts_in.at[mem], 7, device(zz, yy, to)).start()
    parts_in[mem] = part[mine, :]

    ffn_f = xg[mine, :].astype(F32)
    gate_value = jax.nn.sigmoid(jnp.sum(ffn_f * branch_gate[...], axis=-1, keepdims=True))
    arrived(arr2.at[most], 6)
    for t in range(SEQ):
        total = jnp.zeros((16, 128), F32)
        for k in range(TOP):
            total = total + route_weights[k, t] * arr2[routes[k, t]].astype(F32)
        tile32[pl.ds(t * 16, 16), :] = total
    arrived(parts_in.at[pl.ds(0, GROUP - 1)], 7)
    for c in range(16):
        cut = slice(c * 128, (c + 1) * 128)
        dense = parts_in[0, :, cut].astype(F32)
        for g in range(1, GROUP):
            dense = dense + parts_in[g, :, cut].astype(F32)
        out[:, cut] = (mid_s[:, cut] + tile32[pl.ds(c, SEQ, stride=16), :] + gate_value * dense).astype(BF16)

    waited(a_in, 0)
    waited(b_in, 1)
    waited(send1.at[most], 2)
    waited(xg.at[pl.ds(0, SEQ * (GROUP - 1))], 3)
    waited(wbuf.at[pl.ds(0, RING - 1), :, :, left], 4)
    waited(wbuf.at[:, pl.ds(0, RING - 1), :, right], 5)
    waited(send2.at[most], 6)
    waited(part.at[pl.ds(0, SEQ * (GROUP - 1))], 7)


def per_device(
    hidden_in,
    lengths,
    attn_gain,
    query_weight,
    key_weight,
    value_weight,
    score_bias,
    out_weight,
    key_cache,
    value_cache,
    ffn_gain,
    routes,
    route_weights,
    expert_gate,
    expert_up,
    expert_down,
    dense_gate,
    dense_up,
    dense_down,
    branch_gate,
):
    smem = pl.BlockSpec(memory_space=pltpu.SMEM)
    vmem = pl.BlockSpec(memory_space=pltpu.VMEM)
    hbm = pl.BlockSpec(memory_space=pl.ANY)
    routes_t = routes.T
    dma = pltpu.SemaphoreType.DMA
    return tuple(
        pl.pallas_call(
            kernel,
            name="decode_layer",
            out_shape=(
                jax.ShapeDtypeStruct((SEQ, D), BF16),
                jax.ShapeDtypeStruct((SEQ, 128), BF16),
                jax.ShapeDtypeStruct((SEQ, 128), BF16),
            ),
            in_specs=[smem] * 4 + [vmem] * 5 + [hbm] * 12,
            out_specs=(vmem, vmem, vmem),
            scratch_shapes=[
                pltpu.VMEM((D, HEADS * HEAD), BF16),
                pltpu.VMEM((D, 128), BF16),
                pltpu.VMEM((D, 128), BF16),
                pltpu.VMEM((HEADS * HEAD, D), BF16),
                pltpu.VMEM((SEQ, LEN, 128), BF16),
                pltpu.VMEM((SEQ, LEN, 128), BF16),
                pltpu.VMEM((D, EFF), BF16),
                pltpu.VMEM((D, EFF), BF16),
                pltpu.VMEM((EFF, D), BF16),
                pltpu.VMEM((RING, RING, 3 * UNITS, D), BF16),
                pltpu.VMEM((GROUP * SEQ, D), BF16),
                pltpu.VMEM((GROUP * SEQ, D), BF16),
                pltpu.VMEM((GROUP, SEQ, D), BF16),
                pltpu.VMEM((DEV * 16, 128), F32),
                pltpu.VMEM((DEV, 16, 128), BF16),
                pltpu.VMEM((DEV, 16, 128), BF16),
                pltpu.VMEM((DEV, 16, 128), BF16),
                pltpu.VMEM((DEV, 16, 128), BF16),
                pltpu.VMEM((SEQ * HEADS, 128), F32),
                pltpu.VMEM((SEQ * HEADS, 128), F32),
                pltpu.VMEM((128, 256), BF16),
                pltpu.VMEM((SEQ, D), F32),
                dma((3 + HEADS,)),
                dma((SEQ,)),
                dma((SEQ,)),
                dma((3,)),
                dma((3,)),
                dma((8,)),
                dma((8,)),
            ],
            compiler_params=pltpu.CompilerParams(
                collective_id=0, has_side_effects=True, vmem_limit_bytes=60 * 1024 * 1024
            ),
        )(
            lengths,
            score_bias,
            routes_t,
            route_weights.T,
            hidden_in,
            attn_gain.reshape(1, D),
            ffn_gain.reshape(1, D),
            branch_gate.reshape(1, D),
            routes_t,
            query_weight,
            key_weight,
            value_weight,
            out_weight,
            key_cache,
            value_cache,
            expert_gate,
            expert_up,
            expert_down,
            dense_gate.T,
            dense_up.T,
            dense_down.T,
        )
    )


def solution(mesh):
    return jax.shard_map(
        per_device,
        mesh=mesh,
        in_specs=(
            P("ep", None),
            P("ep"),
            P(),
            P(),
            P(),
            P(),
            P(),
            P(),
            P("ep", None, None),
            P("ep", None, None),
            P(),
            P("ep", None),
            P("ep", None),
            P("ep", None, None),
            P("ep", None, None),
            P("ep", None, None),
            P(None, "ep"),
            P(None, "ep"),
            P(None, "ep"),
            P(),
        ),
        out_specs=(P("ep", None), P("ep", None), P("ep", None)),
        check_vma=False,
    )
```

time: 141 us -> 65 us (0.46)
  Pallas kernels: 0 us -> 60.1 us
  matrix products: 38.7 us -> 0 us
  waiting for transfers between devices: 36.5 us -> 0 us
  local copies, waits for them, and re-layouts: 26.8 us -> 4.02 us
  starting transfers between devices: 16 us -> 0 us
  between operations: 14.3 us -> 0.65 us
  other arithmetic: 7.42 us -> 0 us
    pallas_call x0 -> x1, Pallas kernels: none -> 60.1 us  [per_device(): pl.pallas_call(kernel, name='decode_layer', out_shape=(jax.ShapeDtypeStru...]
    dot_general x13 -> x0, matrix products: 38.7 us -> none  [the longest x1 9.79 us: down_product(): lax.dot_general(hidden_rows, down_w, (((1,), (1,)), ((), ())), preferred_...]
    all_to_all x2 -> x0, waiting for transfers between devices: 29.3 us -> none  [the longest x1 15 us: per_device(): lax.all_to_all(expert_rows.reshape(arrived.shape), 'ep', split_axis=0, co...]
    unnamed x33 -> x3, local copies, waits for them, and re-layouts: 23.1 us -> 4.02 us
    all_to_all x2 -> x0, starting transfers between devices: 15.9 us -> none  [the longest x1 11.9 us: per_device(): lax.all_to_all(outgoing, 'ep', split_axis=0, concat_axis=0, tiled=True)]
    all_gather x1 -> x0, waiting for transfers between devices: 7.15 us -> none  [turned_gather(): result, at, done = (lax.all_gather(both, axis, axis=0, tiled=True), 0, [])]
    reshape x2 -> x0, other arithmetic: 3.04 us -> none  [the longest x1 2.05 us: per_device(): expert_rows.reshape(arrived.shape)]
    reduce_sum x4 -> x0, other arithmetic: 1.79 us -> none  [the longest x1 0.97 us: rms_norm(): jnp.mean(as_float * as_float, axis=-1, keepdims=True) + norm_eps]
  transfers between devices with their start and end apart: 3 -> 0, of which waited for: 3 -> 0; matrix products, arithmetic and copies ran while one was open for 40% -> 0% of each run, Pallas kernels for 0% -> 0%
where the time goes in v1:
time: 65 us; the launch traced here: 64.7 us
  Pallas kernels  60.1 us (92%)
  local copies, waits for them, and re-layouts  4.02 us (6%)
  between operations  0.65 us (1%)
    pallas_call x1, Pallas kernels, per_device(): pl.pallas_call(kernel, name='decode_layer', out_shape=(jax.ShapeDtypeStru...  60.1 us
    unnamed x3, local copies, waits for them, and re-layouts  4.02 us

profile of v1, /device:TPU:1, one launch (start us, length us, event | category | flops | bytes accessed | tf_op | source)
XLA Modules:
  0.0 64.7 jit_solution(14124031736847231469)
XLA Ops:
  0.6 60.1 %decode_layer.1 = (bf16[16,2048]{1,0:T(8,128)(2,1)}, bf16[16,128]{1,0:T(8,128)(2,1)}, bf16[16,128]{1,0:T(8,128)(2,1)}) custom-call(s32[16]{0:T(128)} %lens.1, f32[8]{0:T(128)} %bias.1, s32[4,16]{1,0:T(4,128)} %bitcast.14, f32[4,16]{1,0:T(4,128)} %bitcast.16, bf16[16,2048]{1,0:T(8,128)(2,1)} %hid.1, f32[1,2048]{1,0:T(1,128)} %bitcast.11, f32[1,2048]{1,0:T(1,128)} %bitcast.12, ...), custom_call_target="tpu_custom_call" | custom-call | tf_op jit(solution)/shard_map/decode_layer/pallas_call | solution.py:370
  60.7 1.5 %copy.26 = bf16[16,2048]{1,0:T(8,128)(2,1)} copy(bf16[16,2048]{1,0:T(8,128)(2,1)} %get-tuple-element.6) | data formatting | bytes 131072
  62.2 1.3 %copy.27 = bf16[16,128]{1,0:T(8,128)(2,1)} copy(bf16[16,128]{1,0:T(8,128)(2,1)} %get-tuple-element.7) | data formatting | bytes 8192
  63.5 1.3 %copy.28 = bf16[16,128]{1,0:T(8,128)(2,1)} copy(bf16[16,128]{1,0:T(8,128)(2,1)} %get-tuple-element.8) | data formatting | bytes 8192

commit v2 on v1

v2 whole, which is shorter than its diff:
```python
import jax
import jax.numpy as jnp
from jax import lax
from jax.experimental import pallas as pl
from jax.experimental.pallas import tpu as pltpu
from jax.sharding import PartitionSpec as P

AXIS = "ep"
DEV = 128
GROUP = 8
RING = 4
SEQ = 16
D = 2048
LEN = 1024
HEAD = 64
HEADS = 8
TOP = 4
EFF = 512
UNITS = 16
EPS = 1e-06
MESH = pl.DeviceIdType.MESH
BF16 = jnp.bfloat16
F32 = jnp.float32


def rms_norm(values, gain):
    scale = lax.rsqrt(jnp.mean(values * values, axis=-1, keepdims=True) + EPS)
    return (values * scale * gain).astype(BF16)


def silu(v):
    return v / (1.0 + jnp.exp(-v))


def nt_dot(a, b):
    return lax.dot_general(a, b, (((1,), (1,)), ((), ())), preferred_element_type=F32)


def dot(a, b):
    return jnp.dot(a, b, preferred_element_type=F32)


def kernel(
    lens_h,
    bias_h,
    routes_h,
    route_weights_h,
    hid_h,
    attn_gain_h,
    ffn_gain_h,
    branch_gate_h,
    qw_h,
    kw_h,
    vw_h,
    ow_h,
    kc_h,
    vc_h,
    eg_h,
    eu_h,
    ed_h,
    dg_h,
    du_h,
    dd_h,
    out_h,
    new_keys_h,
    new_values_h,
    lens,
    bias,
    routes,
    route_weights,
    hid,
    attn_gain,
    ffn_gain,
    branch_gate,
    routes_v,
    out,
    new_keys,
    new_values,
    qw,
    kw,
    vw,
    ow,
    kc,
    vc,
    eg,
    eu,
    ed,
    wbuf,
    xg,
    part,
    part2,
    pair_in,
    parts_in,
    tile32,
    send1,
    arr1,
    send2,
    arr2,
    qs,
    os_,
    tri,
    mid_s,
    s_sem,
    o_sem,
    w_sem,
    k_sem,
    v_sem,
    e_sem,
    d_sem,
    snd,
    rcv,
    ready,
):
    me = lax.axis_index(AXIS)
    grp = me // GROUP
    mem = lax.rem(me, GROUP)
    zz = grp // RING
    yy = lax.rem(grp, RING)

    def device(z, y, member):
        return ((z * RING + y) * GROUP + member,)

    in_y = [device(zz, lax.rem(yy + d, RING), mem) for d in (1, 3, 2)]
    in_z = [device(lax.rem(zz + d, RING), yy, mem) for d in (1, 3, 2)]
    xx, core = mem // 2, lax.rem(mem, 2)
    in_x = [device(zz, yy, lax.rem(xx + d, RING) * 2 + core) for d in (1, 3, 2)]
    sibling = device(zz, yy, xx * 2 + 1 - core)
    in_group = [device(zz, yy, lax.rem(mem + d, GROUP)) for d in range(1, GROUP)]

    def signal(sem, devices):
        for to in devices:
            pl.semaphore_signal(sem, inc=1, device_id=to, device_id_type=MESH)

    barrier = pltpu.get_barrier_semaphore()
    signal(barrier, in_y + in_z + in_group)

    def copy(src, dst, sem):
        return pltpu.make_async_copy(src, dst, sem)

    own = [
        copy(dg_h, wbuf.at[zz, yy, pl.ds(0, UNITS)], d_sem.at[0]),
        copy(du_h, wbuf.at[zz, yy, pl.ds(UNITS, UNITS)], d_sem.at[1]),
        copy(dd_h, wbuf.at[zz, yy, pl.ds(2 * UNITS, UNITS)], d_sem.at[2]),
    ]
    proj = [copy(qw_h, qw, w_sem.at[0]), copy(kw_h, kw, w_sem.at[1]), copy(vw_h, vw, w_sem.at[2])]
    outw = [
        copy(
            ow_h.at[pl.ds(h * HEAD, HEAD)],
            ow.at[pl.ds((h % 4) * 2 * HEAD + (h // 4) * HEAD, HEAD)],
            w_sem.at[3 + h],
        )
        for h in range(HEADS)
    ]
    experts = [copy(eg_h.at[0], eg, e_sem.at[0]), copy(eu_h.at[0], eu, e_sem.at[1]), copy(ed_h.at[0], ed, e_sem.at[2])]
    first = [copy(hid_h, hid, s_sem.at[0]), copy(attn_gain_h, attn_gain, s_sem.at[1])]
    scalars = [copy(lens_h, lens, s_sem.at[2]), copy(bias_h, bias, s_sem.at[3])]
    later = [
        copy(ffn_gain_h, ffn_gain, s_sem.at[4]),
        copy(branch_gate_h, branch_gate, s_sem.at[5]),
        copy(routes_h, routes, s_sem.at[6]),
        copy(route_weights_h, route_weights, s_sem.at[7]),
        copy(routes_h, routes_v, s_sem.at[8]),
    ]
    results = [copy(out, out_h, o_sem.at[0]), copy(new_keys, new_keys_h, o_sem.at[1]), copy(new_values, new_values_h, o_sem.at[2])]
    for c in own + first + proj + scalars:
        c.start()

    @pl.loop(0, SEQ)
    def _(b):
        copy(kc_h.at[b], kc.at[b], k_sem.at[b]).start()
        copy(vc_h.at[b], vc.at[b], v_sem.at[b]).start()

    for c in later + outw + experts:
        c.start()

    half = D // 2
    left, right = pl.ds(0, half), pl.ds(half, half)

    def remote(src, dst, s, to):
        return pltpu.make_async_remote_copy(
            src_ref=src, dst_ref=dst, send_sem=snd.at[s], recv_sem=rcv.at[s], device_id=to, device_id_type=MESH
        )

    def push(block, s, to):
        remote(block, block, s, to).start()

    def waited(ref, s):
        copy(ref, ref, snd.at[s]).wait()

    def arrived(ref, s):
        with jax.named_scope(f"arrived_{s}"):
            copy(ref, ref, rcv.at[s]).wait()

    def start_weights():
        with jax.named_scope("barrier_1"):
            pl.semaphore_wait(barrier, len(in_y + in_z + in_group))
        signal(ready.at[0], in_y)
        for c in own:
            c.wait()
        for to in in_y:
            push(wbuf.at[zz, yy, :, left], 0, to)
        for to in in_z:
            push(wbuf.at[zz, yy, :, right], 1, to)
        for to in in_z[:2]:
            push(wbuf.at[zz, yy, :, left], 4, to)
        for to in in_y[:2]:
            push(wbuf.at[zz, yy, :, right], 5, to)

    def blocks_of(a, b):
        return wbuf.at[pl.ds(0, a), pl.ds(0, b), :, left]

    z_by = [lax.rem(zz + d, RING) for d in range(RING)]
    y_by = [lax.rem(yy + d, RING) for d in range(RING)]

    @pl.when(zz == 3)
    def _():
        start_weights()

    row = lax.broadcasted_iota(jnp.int32, (128, 256), 0)
    col = lax.broadcasted_iota(jnp.int32, (128, 256), 1)
    tri[...] = jnp.where((row > col) | (col >= 128), 1.0, 0.0).astype(BF16)

    for c in first:
        c.wait()
    normed = rms_norm(hid[...].astype(F32), attn_gain[...])
    for c in proj:
        c.wait()
    new_keys[...] = dot(normed, kw[...]).astype(BF16)
    new_values[...] = dot(normed, vw[...]).astype(BF16)
    for c in results[1:]:
        c.start()
    queries = dot(normed, qw[...]).astype(BF16).astype(F32)
    low = lax.broadcasted_iota(jnp.int32, (SEQ, 128), 1) < HEAD
    for h in range(HEADS):
        piece = queries[:, (h // 2) * 128 : (h // 2 + 1) * 128]
        if (h % 2) != (h // 4):
            piece = pltpu.roll(piece, HEAD, axis=1)
        piece = jnp.where(low, piece, 0.0) if h < 4 else jnp.where(low, 0.0, piece)
        qs[pl.ds(h, SEQ, stride=HEADS), :] = piece

    @pl.when((zz == 1) | (zz == 2))
    def _():
        start_weights()

    for c in scalars:
        c.wait()
    heads = lax.broadcasted_iota(jnp.int32, (HEADS, LEN), 0)
    bias_v = jnp.zeros((HEADS, LEN), F32)
    for h in range(HEADS):
        bias_v = jnp.where(heads == h, bias[h], bias_v)
    pos = lax.broadcasted_iota(jnp.int32, (HEADS, LEN), 1)
    blocks = LEN // 128

    @jax.named_scope("attend")
    def attend(start, count):
        logs, keeps, lives = [], [], []
        for j in range(count):
            b = start + j
            copy(kc_h.at[b], kc.at[b], k_sem.at[b]).wait()
            q = qs[pl.ds(b * HEADS, HEADS), :].astype(BF16)
            z = nt_dot(q, kc[b]) * (HEAD**-0.5) + bias_v
            live = pos < lens[b]
            t = jnp.log(1.0 + jnp.exp(-jnp.abs(z)))
            logs.append(jnp.minimum(z, 0.0) - t)
            keeps.append(jnp.where(live, jnp.minimum(-z, 0.0) - t, 0.0))
            lives.append(live)
        keep = jnp.concatenate(
            [keeps[j][:, c * 128 : (c + 1) * 128] for j in range(count) for c in range(blocks)], axis=0
        )
        hi = keep.astype(BF16)
        rest = keep - hi.astype(F32)
        mid = rest.astype(BF16)
        lo = (rest - mid.astype(F32)).astype(BF16)
        sums = dot(hi, tri[...]) + dot(mid, tri[...]) + dot(lo, tri[...])
        for j in range(count):
            b = start + j
            beyond = jnp.zeros((HEADS, 128), F32)
            pieces = [None] * blocks
            for c in reversed(range(blocks)):
                at = (j * blocks + c) * HEADS
                after = sums[at : at + HEADS, :128] + beyond
                beyond = beyond + sums[at : at + HEADS, 128:]
                cut = slice(c * 128, (c + 1) * 128)
                pieces[c] = jnp.where(lives[j][:, cut], jnp.exp(logs[j][:, cut] + after), 0.0)
            weights = jnp.concatenate(pieces, axis=1).astype(BF16)
            copy(vc_h.at[b], vc.at[b], v_sem.at[b]).wait()
            os_[pl.ds(b * HEADS, HEADS), :] = dot(weights, vc[b])

    attend(0, 8)

    @pl.when(zz == 0)
    def _():
        start_weights()

    attend(8, 4)
    with jax.named_scope("barrier_2"):
        pl.semaphore_wait(ready.at[0], len(in_y))
    signal(ready.at[1], in_group)

    arrived(blocks_of(1, 3), 0)
    arrived(blocks_of(1, 3), 1)
    for d in (1, 2, 3):
        for to in in_z[:2]:
            push(wbuf.at[zz, y_by[d], :, left], 8, to)
        for to in in_y[:2]:
            push(wbuf.at[z_by[d], yy, :, right], 9, to)

    attend(12, 4)
    with jax.named_scope("barrier_3"):
        pl.semaphore_wait(ready.at[1], len(in_group))

    for c in later + outw:
        c.wait()
    attended = []
    for h in range(4):
        first = os_[pl.ds(h, SEQ, stride=HEADS), :]
        second = os_[pl.ds(h + 4, SEQ, stride=HEADS), :]
        attended.append(jnp.where(low, first, second).astype(BF16))
    middle = hid[...].astype(F32) + dot(jnp.concatenate(attended, axis=1), ow[...])
    mid_s[...] = middle
    ffn_in = rms_norm(middle, ffn_gain[...])
    xg[xx, core] = ffn_in

    experts_i = lax.broadcasted_iota(jnp.int32, (DEV, SEQ), 0)
    hit = routes_v[0:1, :] == experts_i
    for k in range(1, TOP):
        hit = hit | (routes_v[k : k + 1, :] == experts_i)
    pick = jnp.where(hit, 1.0, 0.0).astype(BF16)

    def to_rows(values, c):
        for j in range(values.shape[1] // 128):
            tile32[pl.ds(c + j, DEV, stride=16), :] = values[:, j * 128 : (j + 1) * 128]

    def pack(dst):
        @pl.loop(0, DEV // 8)
        def _(i):
            for j in range(8):
                r = i * 8 + j
                dst[r] = tile32[pl.ds(pl.multiple_of(r * 16, 16), 16), :].astype(BF16)

    def exchange(src, dst, s):
        with jax.named_scope(f"exchange_{s}"):

            @pl.loop(1, DEV)
            def _(d):
                t = lax.rem(me + d, DEV)
                remote(src.at[t], dst.at[me], s, (t,)).start()

    for c in range(0, 16, 4):
        to_rows(dot(pick, ffn_in[:, c * 128 : (c + 4) * 128]), c)
    pack(send1)
    exchange(send1, arr1, 2)
    arr1[me] = send1[me]
    for to in in_x:
        push(xg.at[xx, core], 3, to)

    arrived(blocks_of(1, 2), 4)
    arrived(blocks_of(1, 2), 5)
    push(wbuf.at[z_by[3], yy, :, left], 10, in_z[0])
    push(wbuf.at[zz, y_by[3], :, right], 11, in_y[0])
    arrived(blocks_of(2, 3), 8)
    arrived(blocks_of(2, 3), 9)
    for d, side in ((1, 3), (2, 1), (3, 1)):
        push(wbuf.at[z_by[side], y_by[d], :, left], 12, in_z[0 if side == 3 else 1])
        push(wbuf.at[z_by[d], y_by[side], :, right], 13, in_y[0 if side == 3 else 1])

    for c in experts:
        c.wait()
    most = pl.ds(0, DEV - 1)
    arrived(arr1.at[most], 2)
    arrived(xg.at[pl.ds(0, 3), 0], 3)
    push(xg.at[:, core], 14, sibling)

    @pl.loop(0, DEV // 8)
    def _(i):
        for j in range(8):
            r = i * 8 + j
            tile32[pl.ds(pl.multiple_of(r * 16, 16), 16), :] = arr1[r].astype(F32)

    rows = jnp.concatenate([tile32[pl.ds(c, DEV, stride=16), :].astype(BF16) for c in range(16)], axis=1)
    hidden = (silu(dot(rows, eg[...])) * dot(rows, eu[...])).astype(BF16)
    for c in range(0, 16, 4):
        to_rows(dot(hidden, ed[:, c * 128 : (c + 4) * 128]), c)
    pack(send2)

    exchange(send2, arr2, 6)
    arr2[me] = send2[me]

    arrived(xg.at[:, 0], 14)
    arrived(blocks_of(1, 1), 10)
    arrived(blocks_of(1, 1), 11)
    arrived(blocks_of(1, 3), 12)
    arrived(blocks_of(1, 3), 13)
    tokens = xg[...].reshape(GROUP * SEQ, D)

    def share(n):
        return wbuf[:, :, n * UNITS : (n + 1) * UNITS, :].reshape(RING * RING * UNITS, D)

    dense_hidden = (silu(nt_dot(tokens, share(0))) * nt_dot(tokens, share(1))).astype(BF16)
    part[...] = dot(dense_hidden, share(2)).astype(BF16).reshape(RING, 2, SEQ, D)
    remote(part.at[:, 1 - core], pair_in, 15, sibling).start()
    arrived(pair_in, 15)
    for x in range(RING):
        part2[x] = (part[x, core].astype(F32) + pair_in[x].astype(F32)).astype(BF16)
    for d, to in zip((1, 3, 2), in_x):
        remote(part2.at[lax.rem(xx + d, RING)], parts_in.at[xx], 7, to).start()
    parts_in[xx] = part2[xx]

    ffn_f = xg[xx, core].astype(F32)
    gate_value = jax.nn.sigmoid(jnp.sum(ffn_f * branch_gate[...], axis=-1, keepdims=True))
    arrived(arr2.at[most], 6)
    for t in range(SEQ):
        total = jnp.zeros((16, 128), F32)
        for k in range(TOP):
            total = total + route_weights[k, t] * arr2[routes[k, t]].astype(F32)
        tile32[pl.ds(t * 16, 16), :] = total
    arrived(parts_in.at[pl.ds(0, RING - 1)], 7)
    for c in range(16):
        cut = slice(c * 128, (c + 1) * 128)
        dense = parts_in[0, :, cut].astype(F32)
        for g in range(1, RING):
            dense = dense + parts_in[g, :, cut].astype(F32)
        out[:, cut] = (mid_s[:, cut] + tile32[pl.ds(c, SEQ, stride=16), :] + gate_value * dense).astype(BF16)

    results[0].start()

    with jax.named_scope("sent"):
        for n, many in enumerate(
            (
                blocks_of(1, 3),
                blocks_of(1, 3),
                send1.at[most],
                xg.at[pl.ds(0, 3), 0],
                blocks_of(1, 2),
                blocks_of(1, 2),
                send2.at[most],
                part2.at[pl.ds(0, 3)],
                blocks_of(2, 3),
                blocks_of(2, 3),
                blocks_of(1, 1),
                blocks_of(1, 1),
                blocks_of(1, 3),
                blocks_of(1, 3),
                xg.at[:, 0],
                pair_in,
            )
        ):
            waited(many, n)
        for c in results:
            c.wait()


def hand_on(*arrays):
    n = len(arrays)

    def body(*refs):
        ins, outs, held, sem = refs[:n], refs[n : 2 * n], refs[2 * n : 3 * n], refs[3 * n]
        gets = [pltpu.make_async_copy(ins[i], held[i], sem.at[i]) for i in range(n)]
        puts = [pltpu.make_async_copy(held[i], outs[i], sem.at[n + i]) for i in range(n)]
        for c in gets:
            c.start()
        for g, p in zip(gets, puts):
            g.wait()
            p.start()
        for c in puts:
            c.wait()

    spec = pl.BlockSpec(memory_space=pl.ANY)
    return pl.pallas_call(
        body,
        name="hand_on",
        out_shape=tuple(jax.ShapeDtypeStruct(a.shape, a.dtype) for a in arrays),
        in_specs=[spec] * n,
        out_specs=(spec,) * n,
        scratch_shapes=[pltpu.VMEM(a.shape, a.dtype) for a in arrays] + [pltpu.SemaphoreType.DMA((2 * n,))],
        compiler_params=pltpu.CompilerParams(vmem_limit_bytes=60 * 1024 * 1024),
    )(*arrays)


def per_device(
    hidden_in,
    lengths,
    attn_gain,
    query_weight,
    key_weight,
    value_weight,
    score_bias,
    out_weight,
    key_cache,
    value_cache,
    ffn_gain,
    routes,
    route_weights,
    expert_gate,
    expert_up,
    expert_down,
    dense_gate,
    dense_up,
    dense_down,
    branch_gate,
):
    hbm = pl.BlockSpec(memory_space=pl.ANY)
    dma = pltpu.SemaphoreType.DMA
    return hand_on(
        *pl.pallas_call(
            kernel,
            name="decode_layer",
            out_shape=(
                jax.ShapeDtypeStruct((SEQ, D), BF16),
                jax.ShapeDtypeStruct((SEQ, 128), BF16),
                jax.ShapeDtypeStruct((SEQ, 128), BF16),
            ),
            in_specs=[hbm] * 20,
            out_specs=(hbm, hbm, hbm),
            scratch_shapes=[
                pltpu.SMEM((SEQ,), jnp.int32),
                pltpu.SMEM((HEADS,), F32),
                pltpu.SMEM((TOP, SEQ), jnp.int32),
                pltpu.SMEM((TOP, SEQ), F32),
                pltpu.VMEM((SEQ, D), BF16),
                pltpu.VMEM((1, D), F32),
                pltpu.VMEM((1, D), F32),
                pltpu.VMEM((1, D), F32),
                pltpu.VMEM((TOP, SEQ), jnp.int32),
                pltpu.VMEM((SEQ, D), BF16),
                pltpu.VMEM((SEQ, 128), BF16),
                pltpu.VMEM((SEQ, 128), BF16),
                pltpu.VMEM((D, HEADS * HEAD), BF16),
                pltpu.VMEM((D, 128), BF16),
                pltpu.VMEM((D, 128), BF16),
                pltpu.VMEM((HEADS * HEAD, D), BF16),
                pltpu.VMEM((SEQ, LEN, 128), BF16),
                pltpu.VMEM((SEQ, LEN, 128), BF16),
                pltpu.VMEM((D, EFF), BF16),
                pltpu.VMEM((D, EFF), BF16),
                pltpu.VMEM((EFF, D), BF16),
                pltpu.VMEM((RING, RING, 3 * UNITS, D), BF16),
                pltpu.VMEM((RING, 2, SEQ, D), BF16),
                pltpu.VMEM((RING, 2, SEQ, D), BF16),
                pltpu.VMEM((RING, SEQ, D), BF16),
                pltpu.VMEM((RING, SEQ, D), BF16),
                pltpu.VMEM((RING, SEQ, D), BF16),
                pltpu.VMEM((DEV * 16, 128), F32),
                pltpu.VMEM((DEV, 16, 128), BF16),
                pltpu.VMEM((DEV, 16, 128), BF16),
                pltpu.VMEM((DEV, 16, 128), BF16),
                pltpu.VMEM((DEV, 16, 128), BF16),
                pltpu.VMEM((SEQ * HEADS, 128), F32),
                pltpu.VMEM((SEQ * HEADS, 128), F32),
                pltpu.VMEM((128, 256), BF16),
                pltpu.VMEM((SEQ, D), F32),
                dma((9,)),
                dma((3,)),
                dma((3 + HEADS,)),
                dma((SEQ,)),
                dma((SEQ,)),
                dma((3,)),
                dma((3,)),
                dma((16,)),
                dma((16,)),
                pltpu.SemaphoreType.REGULAR((2,)),
            ],
            compiler_params=pltpu.CompilerParams(
                collective_id=0, has_side_effects=True, vmem_limit_bytes=60 * 1024 * 1024
            ),
        )(
            lengths,
            score_bias,
            routes.T,
            route_weights.T,
            hidden_in,
            attn_gain.reshape(1, D),
            ffn_gain.reshape(1, D),
            branch_gate.reshape(1, D),
            query_weight,
            key_weight,
            value_weight,
            out_weight,
            key_cache,
            value_cache,
            expert_gate,
            expert_up,
            expert_down,
            dense_gate.T,
            dense_up.T,
            dense_down.T,
        )
    )


def solution(mesh):
    return jax.shard_map(
        per_device,
        mesh=mesh,
        in_specs=(
            P("ep", None),
            P("ep"),
            P(),
            P(),
            P(),
            P(),
            P(),
            P(),
            P("ep", None, None),
            P("ep", None, None),
            P(),
            P("ep", None),
            P("ep", None),
            P("ep", None, None),
            P("ep", None, None),
            P("ep", None, None),
            P(None, "ep"),
            P(None, "ep"),
            P(None, "ep"),
            P(),
        ),
        out_specs=(P("ep", None), P("ep", None), P("ep", None)),
        check_vma=False,
    )
```

time: 65 us -> 49.1 us (0.76)
  Pallas kernels: 60.1 us -> 48.3 us
  local copies, waits for them, and re-layouts: 4.02 us -> 0 us
    pallas_call x1, Pallas kernels: 60.1 us -> 46.8 us  [per_device(): pl.pallas_call(kernel, name='decode_layer', out_shape=(jax.ShapeDtypeStru...]
    unnamed x3 -> x0, local copies, waits for them, and re-layouts: 4.02 us -> none
    pallas_call x0 -> x1, Pallas kernels: none -> 1.53 us  [hand_on(): pl.pallas_call(body, name='hand_on', out_shape=tuple((jax.ShapeDtypeStruc...]
where the time goes in v2:
time: 49.1 us; the launch traced here: 49 us
  Pallas kernels  48.3 us (98%)
  between operations  0.65 us (1%)
    pallas_call x1, Pallas kernels, per_device(): pl.pallas_call(kernel, name='decode_layer', out_shape=(jax.ShapeDtypeStru...  46.8 us
    pallas_call x1, Pallas kernels, hand_on(): pl.pallas_call(body, name='hand_on', out_shape=tuple((jax.ShapeDtypeStruc...  1.53 us

profile of v2, /device:TPU:1, one launch (start us, length us, event | category | flops | bytes accessed | tf_op | source)
XLA Modules:
  0.0 49.0 jit_solution(6482315817985964795)
XLA Ops:
  0.6 46.8 %decode_layer.1 = (bf16[16,2048]{1,0:T(8,128)(2,1)}, bf16[16,128]{1,0:T(8,128)(2,1)}, bf16[16,128]{1,0:T(8,128)(2,1)}) custom-call(s32[16]{0:T(128)} %lens_h.1, f32[8]{0:T(128)} %bias_h.1, s32[4,16]{1,0:T(4,128)} %bitcast.14, f32[4,16]{1,0:T(4,128)} %bitcast.15, bf16[16,2048]{1,0:T(8,128)(2,1)} %hid_h.1, f32[1,2048]{1,0:T(1,128)} %bitcast.11, ...), custom_call_target="tpu_custom_call" | custom-call | tf_op jit(solution)/shard_map/decode_layer/pallas_call | solution.py:505
  47.5 1.5 %hand_on.1 = (bf16[16,2048]{1,0:T(8,128)(2,1)}, bf16[16,128]{1,0:T(8,128)(2,1)}, bf16[16,128]{1,0:T(8,128)(2,1)}) custom-call(bf16[16,2048]{1,0:T(8,128)(2,1)} %get-tuple-element.6.refs_0_, bf16[16,128]{1,0:T(8,128)(2,1)} %get-tuple-element.7.refs_1_, bf16[16,128]{1,0:T(8,128)(2,1)} %get-tuple-element.8.refs_2_), custom_call_target="tpu_custom_call" | custom-call | tf_op jit(solution)/shard_map/hand_on/pallas_call | solution.py:469

commit v3 on v2

--- a/solution.py
+++ b/solution.py
@@ -1,3 +1,5 @@
+import itertools
+
 import jax
 import jax.numpy as jnp
 from jax import lax
@@ -20,6 +22,10 @@
 EPS = 1e-06
 MESH = pl.DeviceIdType.MESH
 BF16 = jnp.bfloat16
+FAR_FIRST = sorted(
+    (o for o in itertools.product(range(RING), range(RING), range(RING), range(2)) if any(o)),
+    key=lambda o: -sum(min(d, RING - d) for d in o[:3]),
+)
 F32 = jnp.float32
 
 
@@ -165,10 +171,15 @@
     for c in own + first + proj + scalars:
         c.start()
 
-    @pl.loop(0, SEQ)
-    def _(b):
-        copy(kc_h.at[b], kc.at[b], k_sem.at[b]).start()
-        copy(vc_h.at[b], vc.at[b], v_sem.at[b]).start()
+    for first_b in (0, 8):
+
+        @pl.loop(first_b, first_b + 8)
+        def _(b):
+            copy(kc_h.at[b], kc.at[b], k_sem.at[b]).start()
+
+        @pl.loop(first_b, first_b + 8)
+        def _(b):
+            copy(vc_h.at[b], vc.at[b], v_sem.at[b]).start()
 
     for c in later + outw + experts:
         c.start()
@@ -209,6 +220,8 @@
     def blocks_of(a, b):
         return wbuf.at[pl.ds(0, a), pl.ds(0, b), :, left]
 
+    x_by = [lax.rem(xx + d, RING) for d in range(RING)]
+    core_by = [core, 1 - core]
     z_by = [lax.rem(zz + d, RING) for d in range(RING)]
     y_by = [lax.rem(yy + d, RING) for d in range(RING)]
 
@@ -254,9 +267,12 @@
     @jax.named_scope("attend")
     def attend(start, count):
         logs, keeps, lives = [], [], []
+        for b in range(start, start + count):
+            copy(kc_h.at[b], kc.at[b], k_sem.at[b]).wait()
+        for b in range(start, start + count):
+            copy(vc_h.at[b], vc.at[b], v_sem.at[b]).wait()
         for j in range(count):
             b = start + j
-            copy(kc_h.at[b], kc.at[b], k_sem.at[b]).wait()
             q = qs[pl.ds(b * HEADS, HEADS), :].astype(BF16)
             z = nt_dot(q, kc[b]) * (HEAD**-0.5) + bias_v
             live = pos < lens[b]
@@ -283,7 +299,6 @@
                 cut = slice(c * 128, (c + 1) * 128)
                 pieces[c] = jnp.where(lives[j][:, cut], jnp.exp(logs[j][:, cut] + after), 0.0)
             weights = jnp.concatenate(pieces, axis=1).astype(BF16)
-            copy(vc_h.at[b], vc.at[b], v_sem.at[b]).wait()
             os_[pl.ds(b * HEADS, HEADS), :] = dot(weights, vc[b])
 
     attend(0, 8)
@@ -292,22 +307,10 @@
     def _():
         start_weights()
 
-    attend(8, 4)
+    attend(8, 8)
     with jax.named_scope("barrier_2"):
         pl.semaphore_wait(ready.at[0], len(in_y))
     signal(ready.at[1], in_group)
-
-    arrived(blocks_of(1, 3), 0)
-    arrived(blocks_of(1, 3), 1)
-    for d in (1, 2, 3):
-        for to in in_z[:2]:
-            push(wbuf.at[zz, y_by[d], :, left], 8, to)
-        for to in in_y[:2]:
-            push(wbuf.at[z_by[d], yy, :, right], 9, to)
-
-    attend(12, 4)
-    with jax.named_scope("barrier_3"):
-        pl.semaphore_wait(ready.at[1], len(in_group))
 
     for c in later + outw:
         c.wait()
@@ -341,28 +344,42 @@
     def exchange(src, dst, s):
         with jax.named_scope(f"exchange_{s}"):
 
-            @pl.loop(1, DEV)
-            def _(d):
-                t = lax.rem(me + d, DEV)
+            for dz, dy, dx, dc in FAR_FIRST:
+                t = ((z_by[dz] * RING + y_by[dy]) * RING + x_by[dx]) * 2 + core_by[dc]
                 remote(src.at[t], dst.at[me], s, (t,)).start()
 
     for c in range(0, 16, 4):
         to_rows(dot(pick, ffn_in[:, c * 128 : (c + 4) * 128]), c)
     pack(send1)
+    with jax.named_scope("barrier_3"):
+        pl.semaphore_wait(ready.at[1], len(in_group))
+
     exchange(send1, arr1, 2)
     arr1[me] = send1[me]
     for to in in_x:
         push(xg.at[xx, core], 3, to)
 
+    second = {1: (8, 9), 2: (16, 17), 3: (18, 19)}
+    third = {0: (10, 11), 1: (12, 13), 2: (20, 21), 3: (22, 23)}
+
+    arrived(blocks_of(1, 3), 0)
+    arrived(blocks_of(1, 3), 1)
+    for d in (1, 2, 3):
+        for to in in_z[:2]:
+            push(wbuf.at[zz, y_by[d], :, left], second[d][0], to)
+        for to in in_y[:2]:
+            push(wbuf.at[z_by[d], yy, :, right], second[d][1], to)
+
     arrived(blocks_of(1, 2), 4)
     arrived(blocks_of(1, 2), 5)
     push(wbuf.at[z_by[3], yy, :, left], 10, in_z[0])
     push(wbuf.at[zz, y_by[3], :, right], 11, in_y[0])
-    arrived(blocks_of(2, 3), 8)
-    arrived(blocks_of(2, 3), 9)
-    for d, side in ((1, 3), (2, 1), (3, 1)):
-        push(wbuf.at[z_by[side], y_by[d], :, left], 12, in_z[0 if side == 3 else 1])
-        push(wbuf.at[z_by[d], y_by[side], :, right], 13, in_y[0 if side == 3 else 1])
+    def relay(d):
+        arrived(blocks_of(1, 2), second[d][0])
+        arrived(blocks_of(1, 2), second[d][1])
+        side = 3 if d == 1 else 1
+        push(wbuf.at[z_by[side], y_by[d], :, left], third[d][0], in_z[0 if side == 3 else 1])
+        push(wbuf.at[z_by[d], y_by[side], :, right], third[d][1], in_y[0 if side == 3 else 1])
 
     for c in experts:
         c.wait()
@@ -383,27 +400,35 @@
         to_rows(dot(hidden, ed[:, c * 128 : (c + 4) * 128]), c)
     pack(send2)
 
+    for d in (1, 2, 3):
+        relay(d)
+    for n in third[0]:
+        arrived(blocks_of(1, 1), n)
+    for n in third[1]:
+        arrived(blocks_of(1, 1), n)
+    for n in third[2]:
+        arrived(blocks_of(1, 1), n)
     exchange(send2, arr2, 6)
     arr2[me] = send2[me]
 
     arrived(xg.at[:, 0], 14)
-    arrived(blocks_of(1, 1), 10)
-    arrived(blocks_of(1, 1), 11)
-    arrived(blocks_of(1, 3), 12)
-    arrived(blocks_of(1, 3), 13)
+    for n in third[3]:
+        arrived(blocks_of(1, 1), n)
     tokens = xg[...].reshape(GROUP * SEQ, D)
 
     def share(n):
         return wbuf[:, :, n * UNITS : (n + 1) * UNITS, :].reshape(RING * RING * UNITS, D)
 
     dense_hidden = (silu(nt_dot(tokens, share(0))) * nt_dot(tokens, share(1))).astype(BF16)
-    part[...] = dot(dense_hidden, share(2)).astype(BF16).reshape(RING, 2, SEQ, D)
-    remote(part.at[:, 1 - core], pair_in, 15, sibling).start()
-    arrived(pair_in, 15)
-    for x in range(RING):
-        part2[x] = (part[x, core].astype(F32) + pair_in[x].astype(F32)).astype(BF16)
-    for d, to in zip((1, 3, 2), in_x):
-        remote(part2.at[lax.rem(xx + d, RING)], parts_in.at[xx], 7, to).start()
+    for n, cols in enumerate((left, right)):
+        part[:, :, :, cols] = dot(dense_hidden, share(2)[:, n * half : (n + 1) * half]).astype(BF16).reshape(RING, 2, SEQ, half)
+        remote(part.at[:, 1 - core, :, cols], pair_in.at[:, :, cols], (15, 24)[n], sibling).start()
+    for n, cols in enumerate((left, right)):
+        arrived(pair_in.at[:, :, cols], (15, 24)[n])
+        for x in range(RING):
+            part2[x, :, cols] = (part[x, core, :, cols].astype(F32) + pair_in[x, :, cols].astype(F32)).astype(BF16)
+        for d, to in zip((1, 3, 2), in_x):
+            remote(part2.at[x_by[d], :, cols], parts_in.at[xx, :, cols], (7, 25)[n], to).start()
     parts_in[xx] = part2[xx]
 
     ffn_f = xg[xx, core].astype(F32)
@@ -414,8 +439,9 @@
         for k in range(TOP):
             total = total + route_weights[k, t] * arr2[routes[k, t]].astype(F32)
         tile32[pl.ds(t * 16, 16), :] = total
-    arrived(parts_in.at[pl.ds(0, RING - 1)], 7)
     for c in range(16):
+        if c % 8 == 0:
+            arrived(parts_in.at[pl.ds(0, RING - 1), :, (left, right)[c // 8]], (7, 25)[c // 8])
         cut = slice(c * 128, (c + 1) * 128)
         dense = parts_in[0, :, cut].astype(F32)
         for g in range(1, RING):
@@ -434,15 +460,25 @@
                 blocks_of(1, 2),
                 blocks_of(1, 2),
                 send2.at[most],
-                part2.at[pl.ds(0, 3)],
-                blocks_of(2, 3),
-                blocks_of(2, 3),
-                blocks_of(1, 1),
-                blocks_of(1, 1),
-                blocks_of(1, 3),
-                blocks_of(1, 3),
+                part2.at[pl.ds(0, 3), :, left],
+                blocks_of(1, 2),
+                blocks_of(1, 2),
+                blocks_of(1, 1),
+                blocks_of(1, 1),
+                blocks_of(1, 1),
+                blocks_of(1, 1),
                 xg.at[:, 0],
-                pair_in,
+                pair_in.at[:, :, left],
+                blocks_of(1, 2),
+                blocks_of(1, 2),
+                blocks_of(1, 2),
+                blocks_of(1, 2),
+                blocks_of(1, 1),
+                blocks_of(1, 1),
+                blocks_of(1, 1),
+                blocks_of(1, 1),
+                pair_in.at[:, :, left],
+                part2.at[pl.ds(0, 3), :, left],
             )
         ):
             waited(many, n)
@@ -556,8 +592,8 @@
                 dma((SEQ,)),
                 dma((3,)),
                 dma((3,)),
-                dma((16,)),
-                dma((16,)),
+                dma((26,)),
+                dma((26,)),
                 pltpu.SemaphoreType.REGULAR((2,)),
             ],
             compiler_params=pltpu.CompilerParams(

time: 49.1 us -> 46.7 us (0.951); the launches traced: 49 us -> 45.8 us
  Pallas kernels: 48.3 us -> 45.2 us
    pallas_call x1, Pallas kernels: 46.8 us -> 43.7 us  [per_device(): pl.pallas_call(kernel, name='decode_layer', out_shape=(jax.ShapeDtypeStru...]
where the time goes in v3:
time: 46.7 us; the launch traced here: 45.8 us
  Pallas kernels  45.2 us (97%)
  between operations  0.65 us (1%)
    pallas_call x1, Pallas kernels, per_device(): pl.pallas_call(kernel, name='decode_layer', out_shape=(jax.ShapeDtypeStru...  43.7 us
    pallas_call x1, Pallas kernels, hand_on(): pl.pallas_call(body, name='hand_on', out_shape=tuple((jax.ShapeDtypeStruc...  1.53 us

profile of v3, /device:TPU:1, one launch (start us, length us, event | category | flops | bytes accessed | tf_op | source)
XLA Modules:
  0.0 45.8 jit_solution(2427292814064859371)
XLA Ops:
  0.6 43.7 %decode_layer.1 = (bf16[16,2048]{1,0:T(8,128)(2,1)}, bf16[16,128]{1,0:T(8,128)(2,1)}, bf16[16,128]{1,0:T(8,128)(2,1)}) custom-call(s32[16]{0:T(128)} %lens_h.1, f32[8]{0:T(128)} %bias_h.1, s32[4,16]{1,0:T(4,128)} %bitcast.14, f32[4,16]{1,0:T(4,128)} %bitcast.15, bf16[16,2048]{1,0:T(8,128)(2,1)} %hid_h.1, f32[1,2048]{1,0:T(1,128)} %bitcast.11, ...), custom_call_target="tpu_custom_call" | custom-call | tf_op jit(solution)/shard_map/decode_layer/pallas_call | solution.py:541
  44.3 1.5 %hand_on.1 = (bf16[16,2048]{1,0:T(8,128)(2,1)}, bf16[16,128]{1,0:T(8,128)(2,1)}, bf16[16,128]{1,0:T(8,128)(2,1)}) custom-call(bf16[16,2048]{1,0:T(8,128)(2,1)} %get-tuple-element.6.refs_0_, bf16[16,128]{1,0:T(8,128)(2,1)} %get-tuple-element.7.refs_1_, bf16[16,128]{1,0:T(8,128)(2,1)} %get-tuple-element.8.refs_2_), custom_call_target="tpu_custom_call" | custom-call | tf_op jit(solution)/shard_map/hand_on/pallas_call | solution.py:505

commit v4 on v3

--- a/solution.py
+++ b/solution.py
@@ -208,9 +208,9 @@
         signal(ready.at[0], in_y)
         for c in own:
             c.wait()
-        for to in in_y:
+        for to in in_y[:2]:
             push(wbuf.at[zz, yy, :, left], 0, to)
-        for to in in_z:
+        for to in in_z[:2]:
             push(wbuf.at[zz, yy, :, right], 1, to)
         for to in in_z[:2]:
             push(wbuf.at[zz, yy, :, left], 4, to)
@@ -341,34 +341,50 @@
                 r = i * 8 + j
                 dst[r] = tile32[pl.ds(pl.multiple_of(r * 16, 16), 16), :].astype(BF16)
 
-    def exchange(src, dst, s):
+    def exchange(src, dst, s, order=FAR_FIRST):
         with jax.named_scope(f"exchange_{s}"):
 
-            for dz, dy, dx, dc in FAR_FIRST:
+            for dz, dy, dx, dc in order:
                 t = ((z_by[dz] * RING + y_by[dy]) * RING + x_by[dx]) * 2 + core_by[dc]
                 remote(src.at[t], dst.at[me], s, (t,)).start()
 
     for c in range(0, 16, 4):
         to_rows(dot(pick, ffn_in[:, c * 128 : (c + 4) * 128]), c)
     pack(send1)
+    arrived(blocks_of(1, 2), 0)
+    arrived(blocks_of(1, 2), 1)
+    quarter = half // 2
+    push(wbuf.at[zz, y_by[3], :, pl.ds(0, quarter)], 26, in_y[0])
+    push(wbuf.at[zz, y_by[1], :, pl.ds(quarter, quarter)], 26, in_y[1])
+    push(wbuf.at[z_by[3], yy, :, pl.ds(half, quarter)], 27, in_z[0])
+    push(wbuf.at[z_by[1], yy, :, pl.ds(half + quarter, quarter)], 27, in_z[1])
+
     with jax.named_scope("barrier_3"):
         pl.semaphore_wait(ready.at[1], len(in_group))
 
-    exchange(send1, arr1, 2)
+    second = {1: (8, 9), 2: (16, 17), 3: (18, 19)}
+    third = {0: (10, 11), 1: (12, 13), 2: (20, 21), 3: (22, 23)}
+
+    exchange(send1, arr1, 2, FAR_FIRST[:42])
     arr1[me] = send1[me]
+    for to in in_z[:2]:
+        push(wbuf.at[zz, y_by[1], :, left], second[1][0], to)
+    for to in in_y[:2]:
+        push(wbuf.at[z_by[1], yy, :, right], second[1][1], to)
+    exchange(send1, arr1, 2, FAR_FIRST[42:85])
+    for to in in_z[:2]:
+        push(wbuf.at[zz, y_by[3], :, left], second[3][0], to)
+    for to in in_y[:2]:
+        push(wbuf.at[z_by[3], yy, :, right], second[3][1], to)
+    exchange(send1, arr1, 2, FAR_FIRST[85:])
+    arrived(blocks_of(1, 1), 26)
+    arrived(blocks_of(1, 1), 27)
+    for to in in_z[:2]:
+        push(wbuf.at[zz, y_by[2], :, left], second[2][0], to)
+    for to in in_y[:2]:
+        push(wbuf.at[z_by[2], yy, :, right], second[2][1], to)
     for to in in_x:
         push(xg.at[xx, core], 3, to)
-
-    second = {1: (8, 9), 2: (16, 17), 3: (18, 19)}
-    third = {0: (10, 11), 1: (12, 13), 2: (20, 21), 3: (22, 23)}
-
-    arrived(blocks_of(1, 3), 0)
-    arrived(blocks_of(1, 3), 1)
-    for d in (1, 2, 3):
-        for to in in_z[:2]:
-            push(wbuf.at[zz, y_by[d], :, left], second[d][0], to)
-        for to in in_y[:2]:
-            push(wbuf.at[z_by[d], yy, :, right], second[d][1], to)
 
     arrived(blocks_of(1, 2), 4)
     arrived(blocks_of(1, 2), 5)
@@ -381,6 +397,9 @@
         push(wbuf.at[z_by[side], y_by[d], :, left], third[d][0], in_z[0 if side == 3 else 1])
         push(wbuf.at[z_by[d], y_by[side], :, right], third[d][1], in_y[0 if side == 3 else 1])
 
+    relay(1)
+    relay(3)
+
     for c in experts:
         c.wait()
     most = pl.ds(0, DEV - 1)
@@ -400,18 +419,17 @@
         to_rows(dot(hidden, ed[:, c * 128 : (c + 4) * 128]), c)
     pack(send2)
 
-    for d in (1, 2, 3):
-        relay(d)
+    relay(2)
     for n in third[0]:
         arrived(blocks_of(1, 1), n)
     for n in third[1]:
         arrived(blocks_of(1, 1), n)
+    exchange(send2, arr2, 6)
+    arr2[me] = send2[me]
+
+    arrived(xg.at[:, 0], 14)
     for n in third[2]:
         arrived(blocks_of(1, 1), n)
-    exchange(send2, arr2, 6)
-    arr2[me] = send2[me]
-
-    arrived(xg.at[:, 0], 14)
     for n in third[3]:
         arrived(blocks_of(1, 1), n)
     tokens = xg[...].reshape(GROUP * SEQ, D)
@@ -453,8 +471,8 @@
     with jax.named_scope("sent"):
         for n, many in enumerate(
             (
-                blocks_of(1, 3),
-                blocks_of(1, 3),
+                blocks_of(1, 2),
+                blocks_of(1, 2),
                 send1.at[most],
                 xg.at[pl.ds(0, 3), 0],
                 blocks_of(1, 2),
@@ -479,6 +497,8 @@
                 blocks_of(1, 1),
                 pair_in.at[:, :, left],
                 part2.at[pl.ds(0, 3), :, left],
+                blocks_of(1, 1),
+                blocks_of(1, 1),
             )
         ):
             waited(many, n)
@@ -592,8 +612,8 @@
                 dma((SEQ,)),
                 dma((3,)),
                 dma((3,)),
-                dma((26,)),
-                dma((26,)),
+                dma((28,)),
+                dma((28,)),
                 pltpu.SemaphoreType.REGULAR((2,)),
             ],
             compiler_params=pltpu.CompilerParams(

time: 46.7 us -> 46 us (0.985); the launches traced: 45.8 us -> 45.8 us
  no operation moved by 1% of the time
where the time goes in v4:
time: 46 us; the launch traced here: 45.8 us
  Pallas kernels  45.2 us (98%)
  between operations  0.65 us (1%)
    pallas_call x1, Pallas kernels, per_device(): pl.pallas_call(kernel, name='decode_layer', out_shape=(jax.ShapeDtypeStru...  43.6 us
    pallas_call x1, Pallas kernels, hand_on(): pl.pallas_call(body, name='hand_on', out_shape=tuple((jax.ShapeDtypeStruc...  1.53 us

profile of v4, /device:TPU:1, one launch (start us, length us, event | category | flops | bytes accessed | tf_op | source)
XLA Modules:
  0.0 45.8 jit_solution(8331951668170659876)
XLA Ops:
  0.6 43.6 %decode_layer.1 = (bf16[16,2048]{1,0:T(8,128)(2,1)}, bf16[16,128]{1,0:T(8,128)(2,1)}, bf16[16,128]{1,0:T(8,128)(2,1)}) custom-call(s32[16]{0:T(128)} %lens_h.1, f32[8]{0:T(128)} %bias_h.1, s32[4,16]{1,0:T(4,128)} %bitcast.14, f32[4,16]{1,0:T(4,128)} %bitcast.15, bf16[16,2048]{1,0:T(8,128)(2,1)} %hid_h.1, f32[1,2048]{1,0:T(1,128)} %bitcast.11, ...), custom_call_target="tpu_custom_call" | custom-call | tf_op jit(solution)/shard_map/decode_layer/pallas_call | solution.py:561
  44.3 1.5 %hand_on.1 = (bf16[16,2048]{1,0:T(8,128)(2,1)}, bf16[16,128]{1,0:T(8,128)(2,1)}, bf16[16,128]{1,0:T(8,128)(2,1)}) custom-call(bf16[16,2048]{1,0:T(8,128)(2,1)} %get-tuple-element.6.refs_0_, bf16[16,128]{1,0:T(8,128)(2,1)} %get-tuple-element.7.refs_1_, bf16[16,128]{1,0:T(8,128)(2,1)} %get-tuple-element.8.refs_2_), custom_call_target="tpu_custom_call" | custom-call | tf_op jit(solution)/shard_map/hand_on/pallas_call | solution.py:525

commit v5 on v4

--- a/solution.py
+++ b/solution.py
@@ -167,7 +167,8 @@
         copy(route_weights_h, route_weights, s_sem.at[7]),
         copy(routes_h, routes_v, s_sem.at[8]),
     ]
-    results = [copy(out, out_h, o_sem.at[0]), copy(new_keys, new_keys_h, o_sem.at[1]), copy(new_values, new_values_h, o_sem.at[2])]
+    results = [copy(out.at[:, pl.ds(n, D // 2)], out_h.at[:, pl.ds(n, D // 2)], o_sem.at[n * 2 // D]) for n in (0, D // 2)]
+    results += [copy(new_keys, new_keys_h, o_sem.at[2]), copy(new_values, new_values_h, o_sem.at[3])]
     for c in own + first + proj + scalars:
         c.start()
 
@@ -240,7 +241,7 @@
         c.wait()
     new_keys[...] = dot(normed, kw[...]).astype(BF16)
     new_values[...] = dot(normed, vw[...]).astype(BF16)
-    for c in results[1:]:
+    for c in results[2:]:
         c.start()
     queries = dot(normed, qw[...]).astype(BF16).astype(F32)
     low = lax.broadcasted_iota(jnp.int32, (SEQ, 128), 1) < HEAD
@@ -465,8 +466,8 @@
         for g in range(1, RING):
             dense = dense + parts_in[g, :, cut].astype(F32)
         out[:, cut] = (mid_s[:, cut] + tile32[pl.ds(c, SEQ, stride=16), :] + gate_value * dense).astype(BF16)
-
-    results[0].start()
+        if c % 8 == 7:
+            results[c // 8].start()
 
     with jax.named_scope("sent"):
         for n, many in enumerate(
@@ -606,7 +607,7 @@
                 pltpu.VMEM((128, 256), BF16),
                 pltpu.VMEM((SEQ, D), F32),
                 dma((9,)),
-                dma((3,)),
+                dma((4,)),
                 dma((3 + HEADS,)),
                 dma((SEQ,)),
                 dma((SEQ,)),

time: 46 us -> 46 us (level)
  no operation moved by 1% of the time
where the time goes in v5:
time: 46 us; the launch traced here: 45.8 us
  Pallas kernels  45.2 us (98%)
  between operations  0.65 us (1%)
    pallas_call x1, Pallas kernels, per_device(): pl.pallas_call(kernel, name='decode_layer', out_shape=(jax.ShapeDtypeStru...  43.6 us
    pallas_call x1, Pallas kernels, hand_on(): pl.pallas_call(body, name='hand_on', out_shape=tuple((jax.ShapeDtypeStruc...  1.53 us

profile of v5, /device:TPU:1, one launch (start us, length us, event | category | flops | bytes accessed | tf_op | source)
XLA Modules:
  0.0 45.8 jit_solution(8367919798600103628)
XLA Ops:
  0.6 43.6 %decode_layer.1 = (bf16[16,2048]{1,0:T(8,128)(2,1)}, bf16[16,128]{1,0:T(8,128)(2,1)}, bf16[16,128]{1,0:T(8,128)(2,1)}) custom-call(s32[16]{0:T(128)} %lens_h.1, f32[8]{0:T(128)} %bias_h.1, s32[4,16]{1,0:T(4,128)} %bitcast.14, f32[4,16]{1,0:T(4,128)} %bitcast.15, bf16[16,2048]{1,0:T(8,128)(2,1)} %hid_h.1, f32[1,2048]{1,0:T(1,128)} %bitcast.11, ...), custom_call_target="tpu_custom_call" | custom-call | tf_op jit(solution)/shard_map/decode_layer/pallas_call | solution.py:562
  44.3 1.5 %hand_on.1 = (bf16[16,2048]{1,0:T(8,128)(2,1)}, bf16[16,128]{1,0:T(8,128)(2,1)}, bf16[16,128]{1,0:T(8,128)(2,1)}) custom-call(bf16[16,2048]{1,0:T(8,128)(2,1)} %get-tuple-element.6.refs_0_, bf16[16,128]{1,0:T(8,128)(2,1)} %get-tuple-element.7.refs_1_, bf16[16,128]{1,0:T(8,128)(2,1)} %get-tuple-element.8.refs_2_), custom_call_target="tpu_custom_call" | custom-call | tf_op jit(solution)/shard_map/hand_on/pallas_call | solution.py:526
